TPU v7x, 128 devices: a whole 4x4x4 slice. The times are simulated.
128 devices in a mesh: rep: 2 (over z_hi), fs: 32 (over z_lo, y, x), tp: 2 (over core).
Axes of the slice: x: 4, y: 4, z: 4 (z_hi: 2, z_lo: 2; z = z_hi * 2 + z_lo), core: 2. Of those that a mesh axis runs over, the one named last changes fastest.
Arguments:
- tokens: bfloat16 [40960, 2048], P(('rep', 'fs', 'tp')), may hold values from -6 to 6
- mix_gain: float32 [2048], replicated, may hold values from 0.1 to 1.9
- w_bgate: bfloat16 [2048, 2048], P('fs', 'tp'), may hold values from -0.125 to 0.125
- w_cgate: bfloat16 [2048, 2048], P('fs', 'tp'), may hold values from -0.125 to 0.125
- w_value: bfloat16 [2048, 2048], P('fs', 'tp'), may hold values from -0.125 to 0.125
- conv_taps: float32 [3, 2048], replicated, may hold values from -3 to 3
- w_mixout: bfloat16 [2048, 2048], P('tp', 'fs'), may hold values from -0.125 to 0.125
- mlp_gain: float32 [2048], replicated, may hold values from 0.1 to 1.9
- w_gate: bfloat16 [2048, 2816], P('fs', 'tp'), may hold values from -0.125 to 0.125
- w_up: bfloat16 [2048, 2816], P('fs', 'tp'), may hold values from -0.125 to 0.125
- w_down: bfloat16 [2816, 2048], P('tp', 'fs'), may hold values from -0.109375 to 0.109375
Outputs:
- block_out: bfloat16 [40960, 2048], P(('rep', 'fs', 'tp'))
All inputs are finite; a program needn't handle non-finite values.
Results may differ from a plain program's by a relative error of at most 0.0085.
Values may be sent and summed in bfloat16 or wider, within the bound.
A program may use at most 128 MiB of HBM per device.

v0:
```python
import jax
import jax.numpy as jnp
from jax import lax
from jax.sharding import Mesh
from jax.sharding import PartitionSpec as P

FS = ("fs_0", "fs_1", "fs_2")
REP_FS_TP = ("rep", "fs_0", "fs_1", "fs_2", "tp")


def sent_to_all(array, axis):
    peers = lax.axis_size(axis)
    return lax.all_to_all(
        jnp.broadcast_to(array[None], (peers, *array.shape)), axis, 0, 0, tiled=True
    )


def in_order(blocks, dim):
    dims = list(blocks.shape[1:])
    dims[dim] *= blocks.shape[0]
    return jnp.moveaxis(blocks, 0, dim).reshape(dims)


def collect(array, axis, dim):
    blocks = sent_to_all(array, axis)
    return in_order(blocks, dim)


def stacked_from(array, axes, turns):
    blocks = array
    for k in turns:
        blocks = lax.all_gather(blocks, axes[k])
    done = turns[::-1]
    back = [done.index(k) for k in range(len(axes))]
    blocks = blocks.transpose(*back, *range(len(axes), blocks.ndim))
    return blocks.reshape(-1, *array.shape)


def gather_axes(array, axes, turns, dim):
    return in_order(stacked_from(array, axes, turns), dim)


def split_up(array, dim, peers):
    dims = array.shape
    blocks = array.reshape(*dims[:dim], peers, dims[dim] // peers, *dims[dim + 1 :])
    return jnp.moveaxis(blocks, dim, 0)


def summed_on_arrival(array, axis, dim):
    blocks = split_up(array, dim, lax.axis_size(axis))
    arrived = lax.all_to_all(blocks, axis, split_axis=0, concat_axis=0, tiled=True)
    return arrived.astype(jnp.float32).sum(axis=0)


def rms_scale(matrix, gain):
    values = matrix.astype(jnp.float32)
    factor = lax.rsqrt(jnp.mean(values * values, axis=-1, keepdims=True) + 1e-06)
    return values * factor * gain


def causal_taps(mixed, filters):
    length = mixed.shape[-2]
    widths = [(0, 0)] * (mixed.ndim - 2) + [(2, 0), (0, 0)]
    padded = jnp.pad(mixed, widths)
    return (
        filters[0] * padded[..., 0:length, :]
        + filters[1] * padded[..., 1 : length + 1, :]
        + filters[2] * padded[..., 2 : length + 2, :]
    )


def gather_rows(normed):
    return collect(normed, "tp", 0)


def project_in(gathered, stacked):
    return jnp.einsum(
        "td,kdc->ktc",
        gathered,
        lax.all_gather(stacked, FS, axis=1, tiled=True),
        preferred_element_type=jnp.float32,
    )


def collect_out(weight):
    return gather_axes(weight, FS, (0, 1, 2), 1)


def sum_parts(local_cols, weight):
    return summed_on_arrival(
        jnp.dot(local_cols, weight, preferred_element_type=jnp.float32).astype(jnp.bfloat16),
        "tp",
        0,
    )


def on_device(
    tokens, mix_gain, w_bgate, w_cgate, w_value, conv_taps, w_mixout, mlp_gain, w_gate, w_up, w_down
):
    normed = rms_scale(tokens, mix_gain).astype(jnp.bfloat16)
    gathered = gather_rows(normed)
    projected = project_in(gathered, jnp.stack([w_bgate, w_cgate, w_value])).astype(jnp.bfloat16)
    channels = projected.shape[2]
    channel_taps = lax.dynamic_slice_in_dim(conv_taps, lax.axis_index("tp") * channels, channels, 1)
    mixed_in = projected[1].astype(jnp.float32) * projected[2].astype(jnp.float32)
    gated = (projected[0].astype(jnp.float32) * causal_taps(mixed_in, channel_taps)).astype(
        jnp.bfloat16
    )
    residual = tokens.astype(jnp.float32) + sum_parts(gated, collect_out(w_mixout))
    normed_two = rms_scale(residual, mlp_gain).astype(jnp.bfloat16)
    gathered_two = gather_rows(normed_two)
    gate_up = project_in(gathered_two, jnp.stack([w_gate, w_up]))
    hidden = (jax.nn.silu(gate_up[0]) * gate_up[1]).astype(jnp.bfloat16)
    result = residual + 0.5 * sum_parts(hidden, collect_out(w_down))
    return result.astype(jnp.bfloat16)


def solution(mesh):
    finer = Mesh(
        mesh.devices.reshape(mesh.shape["rep"], 2, 4, 4, mesh.shape["tp"]),
        ("rep", "fs_0", "fs_1", "fs_2", "tp"),
    )
    return jax.shard_map(
        on_device,
        mesh=finer,
        in_specs=(
            P(REP_FS_TP, None),
            P(),
            P(FS, "tp"),
            P(FS, "tp"),
            P(FS, "tp"),
            P(),
            P("tp", FS),
            P(),
            P(FS, "tp"),
            P(FS, "tp"),
            P("tp", FS),
        ),
        out_specs=P(REP_FS_TP, None),
        check_vma=False,
    )
```

profile of v0, /device:TPU:1, one launch (start us, length us, event | category | flops | bytes accessed | tf_op | source)
XLA Modules:
  0.0 567.4 jit_solution(2443627094710564930)
XLA Ops:
  6.5 6.7 %all-gather = bf16[2048,64]{0,1:T(8,128)(2,1)S(1)} all-gather(bf16[1024,64]{0,1:T(8,128)(2,1)} %param.17), channel_id=2, replica_groups=mesh['rep'=2,'fs_0'=2,'fs_1'=4,'fs_2'=4,'tp'=2] {'fs_0'}, dimensions={0}, use_global_device_ids=true | all-gather | bytes 393216 | tf_op jit(solution)/shard_map/all_gather | solution.py:32
  13.3 0.7 copy.27
  14.1 5.9 %all-gather.3 = bf16[2816,64]{0,1:T(8,128)(2,1)S(1)} all-gather(bf16[1408,64]{0,1:T(8,128)(2,1)} %param.21), channel_id=5, replica_groups=mesh['rep'=2,'fs_0'=2,'fs_1'=4,'fs_2'=4,'tp'=2] {'fs_0'}, dimensions={0}, use_global_device_ids=true | all-gather | bytes 540672 | tf_op jit(solution)/shard_map/all_gather | solution.py:32
  20.0 0.8 copy.26
  20.8 18.1 %all-gather.17.cloned.1.call-done = bf16[8,1024,64]{1,2,0:T(8,128)(2,1)} async-done(((bf16[2,1024,64]{1,2,0:T(8,128)(2,1)}), bf16[8,1024,64]{1,2,0:T(8,128)(2,1)}) %all-gather.17.cloned.1.call-update) | async-done | bytes 1048592 | tf_op jit(solution)/shard_map/all_gather | solution.py:32
  39.0 29.2 %all-gather.21.cloned.1.call-done = bf16[8,1408,64]{1,2,0:T(8,128)(2,1)} async-done(((bf16[2,1408,64]{1,2,0:T(8,128)(2,1)}), bf16[8,1408,64]{1,2,0:T(8,128)(2,1)}) %all-gather.21.cloned.1.call-update) | async-done | bytes 1441808 | tf_op jit(solution)/shard_map/all_gather | solution.py:32
  68.4 0.8 pad_maximum_fusion
  69.3 0.8 pad_maximum_fusion.1
  70.8 1.9 broadcast_in_dim.4
  72.7 4.7 all-to-all-start
  77.4 0.9 constant_dynamic-slice_fusion
  78.3 40.2 %all-gather.19.cloned.1.call-done = bf16[16,2,1024,64]{2,3,1,0:T(8,128)(2,1)} async-done(((bf16[4,2,1024,64]{2,3,1,0:T(8,128)(2,1)}), bf16[16,2,1024,64]{2,3,1,0:T(8,128)(2,1)}) %all-gather.19.cloned.1.call-update) | async-done | bytes 4194320 | tf_op jit(solution)/shard_map/all_gather | solution.py:32
  118.5 4.9 copy.19
  123.4 58.3 %all-gather.23.cloned.1.call-done = bf16[16,2,1408,64]{2,3,1,0:T(8,128)(2,1)} async-done(((bf16[4,2,1408,64]{2,3,1,0:T(8,128)(2,1)}), bf16[16,2,1408,64]{2,3,1,0:T(8,128)(2,1)}) %all-gather.23.cloned.1.call-update) | async-done | bytes 5767184 | tf_op jit(solution)/shard_map/all_gather | solution.py:32
  181.7 5.7 %copy.21 = bf16[2,4,4,1408,64]{3,4,2,1,0:T(8,128)(2,1)} copy(bf16[2,4,4,1408,64]{3,4,0,1,2:T(8,128)(2,1)} %bitcast.63) | data formatting | bytes 11534336 | tf_op jit(solution)/shard_map/transpose | solution.py:35
  187.4 153.6 %all-gather.13.cloned.1.call-done = bf16[3,2048,1024]{2,1,0:T(8,128)(2,1)} async-done(((bf16[3,64,1024]{2,1,0:T(8,128)(2,1)}), bf16[3,2048,1024]{2,1,0:T(8,128)(2,1)}) %all-gather.13.cloned.1.call-update) | async-done | bytes 12582928 | tf_op jit(solution)/shard_map/all_gather | solution.py:80
  341.0 11.2 %convert_bitcast_fusion = bf16[3,640,1024]{2,1,0:T(8,128)(2,1)S(1)} fusion(bf16[640,2048,1]{1,0,2:T(8,128)(2,1)S(1)} %bitcast.67, bf16[3,2048,1024]{2,1,0:T(8,128)(2,1)} %all-gather.13.cloned.1.call-done), kind=kOutput, calls=%fused_computation.3 | convolution fusion | flops 8055029760 | bytes 19136512 | tf_op jit(solution)/shard_map/td,kdc->ktc/dot_general | solution.py:77
  352.2 0.5 multiply_bitcast_fusion
  352.8 1.7 copy-done.3
  354.4 3.5 convolution_convert_fusion.1
  357.9 23.8 %all_to_all.20 = bf16[2,320,2048]{2,1,0:T(8,128)(2,1)S(1)} all-to-all(bf16[2,320,2048]{2,1,0:T(8,128)(2,1)S(1)} %bitcast.68), channel_id=1, replica_groups=mesh['rep'=2,'fs_0'=2,'fs_1'=4,'fs_2'=4,'tp'=2] {'tp'}, dimensions={0} | all-to-all | bytes 5242880 | tf_op jit(solution)/shard_map/all_to_all | solution.py:51
  381.7 0.6 convert_reduce_fusion.1
  382.3 0.7 copy-done.1
  384.2 1.9 broadcast_in_dim.5
  386.1 5.4 all-to-all-start.2
  391.5 120.2 %all-gather.15.cloned.1.call-done = bf16[2,2048,1408]{2,1,0:T(8,128)(2,1)} async-done(((bf16[2,64,1408]{2,1,0:T(8,128)(2,1)}), bf16[2,2048,1408]{2,1,0:T(8,128)(2,1)}) %all-gather.15.cloned.1.call-update) | async-done | bytes 11534352 | tf_op jit(solution)/shard_map/all_gather | solution.py:80
  511.6 13.1 %convolution_bitcast_fusion = f32[2,640,1408]{1,2,0:T(8,128)S(1)} fusion(bf16[2,2048,1408]{2,1,0:T(8,128)(2,1)} %all-gather.15.cloned.1.call-done, bf16[640,2048,1]{1,0,2:T(8,128)(2,1)} %bitcast.21), kind=kOutput, calls=%fused_computation.2 | convolution fusion | flops 7381975040 | bytes 21364736 | tf_op jit(solution)/shard_map/td,kdc->ktc/dot_general | solution.py:77
  524.7 7.0 %convolution_convert_fusion = bf16[640,2048]{1,0:T(8,128)(2,1)S(1)} fusion(bf16[1408,2048]{0,1:T(8,128)(2,1)} %bitcast.64, f32[2,640,1408]{1,2,0:T(8,128)S(1)} %convolution_bitcast_fusion), kind=kOutput, calls=%fused_computation.9 | convolution fusion | flops 3697704960 | bytes 15597568 | tf_op jit(solution)/shard_map/dot_general | solution.py:91
  531.7 25.7 %all_to_all.21 = bf16[2,320,2048]{2,1,0:T(8,128)(2,1)S(1)} all-to-all(bf16[2,320,2048]{2,1,0:T(8,128)(2,1)S(1)} %bitcast.69), channel_id=1, replica_groups=mesh['rep'=2,'fs_0'=2,'fs_1'=4,'fs_2'=4,'tp'=2] {'tp'}, dimensions={0} | all-to-all | bytes 5242880 | tf_op jit(solution)/shard_map/all_to_all | solution.py:51
  557.5 0.6 convert_reduce_fusion
  558.1 0.7 copy-done.2
  558.8 1.8 add_convert_fusion
  (39 shorter events, 2.2 us)
Async XLA Ops:
  6.5 61.8 %copy-start.8 = (bf16[64,1024]{1,0:T(8,128)(2,1)S(1)}, bf16[64,1024]{1,0:T(8,128)(2,1)}, u32[]{:S(2)}) copy-start(bf16[64,1024]{1,0:T(8,128)(2,1)} %param.13) | copy-start | bytes 393220
  6.5 61.8 %copy-start.7 = (bf16[64,1024]{1,0:T(8,128)(2,1)S(1)}, bf16[64,1024]{1,0:T(8,128)(2,1)}, u32[]{:S(2)}) copy-start(bf16[64,1024]{1,0:T(8,128)(2,1)} %param.14) | copy-start | bytes 393220
  6.5 61.8 %copy-start.6 = (bf16[64,1024]{1,0:T(8,128)(2,1)S(1)}, bf16[64,1024]{1,0:T(8,128)(2,1)}, u32[]{:S(2)}) copy-start(bf16[64,1024]{1,0:T(8,128)(2,1)} %param.15) | copy-start | bytes 393220
  6.5 32.4 %all-gather.17.cloned.1.call-start = ((), (), s32[]{:S(2)}) async-start(), calls=%async_computation.6 | async-start | bytes 1310720 | tf_op jit(solution)/shard_map/all_gather | solution.py:32
  14.0 55.2 %copy-start.4 = (bf16[64,1408]{1,0:T(8,128)(2,1)S(1)}, bf16[64,1408]{1,0:T(8,128)(2,1)}, u32[]{:S(2)}) copy-start(bf16[64,1408]{1,0:T(8,128)(2,1)} %param.20) | copy-start | bytes 540676
  14.0 55.2 %copy-start.5 = (bf16[64,1408]{1,0:T(8,128)(2,1)S(1)}, bf16[64,1408]{1,0:T(8,128)(2,1)}, u32[]{:S(2)}) copy-start(bf16[64,1408]{1,0:T(8,128)(2,1)} %param.19) | copy-start | bytes 540676
  14.0 54.2 %all-gather.21.cloned.1.call-start = ((), (), s32[]{:S(2)}) async-start(), calls=%async_computation.8 | async-start | bytes 1802240 | tf_op jit(solution)/shard_map/all_gather | solution.py:32
  20.7 49.4 %copy-start = (bf16[320,2048]{1,0:T(8,128)(2,1)S(1)}, bf16[320,2048]{1,0:T(8,128)(2,1)}, u32[]{:S(2)}) copy-start(bf16[320,2048]{1,0:T(8,128)(2,1)} %param.11) | copy-start | bytes 3932164
  20.7 97.8 %all-gather.19.cloned.1.call-start = ((), (), s32[]{:S(2)}) async-start(), calls=%async_computation.7 | async-start | bytes 5242880 | tf_op jit(solution)/shard_map/all_gather | solution.py:32
  39.0 31.5 %copy-start.9 = (f32[2048]{0:T(1024)S(1)}, f32[2048]{0:T(1024)}, u32[]{:S(2)}) copy-start(f32[2048]{0:T(1024)} %param.12) | copy-start | bytes 24580
  39.0 142.7 %all-gather.23.cloned.1.call-start = ((), (), s32[]{:S(2)}) async-start(), calls=%async_computation.9 | async-start | bytes 7208960 | tf_op jit(solution)/shard_map/all_gather | solution.py:32
  68.3 272.7 %all-gather.13.cloned.1.call-start = ((), (), s32[]{:S(2)}) async-start(), calls=%async_computation.4 | async-start | bytes 12976128 | tf_op jit(solution)/shard_map/all_gather | solution.py:80
  69.2 442.4 %all-gather.15.cloned.1.call-start = ((), (), s32[]{:S(2)}) async-start(), calls=%async_computation.5 | async-start | bytes 11894784 | tf_op jit(solution)/shard_map/all_gather | solution.py:80
  72.7 114.7 %all-to-all-start = ((bf16[2,320,2048]{2,1,0:T(8,128)(2,1)}), bf16[2,320,2048]{2,1,0:T(8,128)(2,1)S(1)}, u32[]{:S(2)}, u32[]{:S(2)}) async-start(bf16[2,320,2048]{2,1,0:T(8,128)(2,1)} %broadcast_in_dim.4), calls=%async_computation | async-start | bytes 5242880 | tf_op jit(solution)/shard_map/all_to_all | solution.py:13
  352.2 2.2 copy-start.3
  381.7 1.3 copy-start.1
  383.0 0.7 copy-start.10
  386.1 125.5 %all-to-all-start.2 = ((bf16[2,320,2048]{2,1,0:T(8,128)(2,1)}), bf16[2,320,2048]{2,1,0:T(8,128)(2,1)}, u32[]{:S(2)}, u32[]{:S(2)}) async-start(bf16[2,320,2048]{2,1,0:T(8,128)(2,1)} %broadcast_in_dim.5), calls=%async_computation.2 | async-start | bytes 5242880 | tf_op jit(solution)/shard_map/all_to_all | solution.py:13
  557.5 1.3 copy-start.2
Sparse Core Ops, SparseCore 0:
  14.1 24.7 all-gather.16
  40.6 27.6 all-gather.20
  69.9 48.5 all-gather.18
  120.0 61.5 all-gather.22
  183.1 157.7 all-gather.12
  342.5 169.0 all-gather.14
where the time goes:
time: 568 us; the launch traced here: 567 us
  waiting for transfers between devices  420 us (74%)
  blocking collectives  62.1 us (11%)
  matrix products  34.9 us (6%)
  local copies, waits for them, and re-layouts  20.1 us (4%)
  between operations  13.6 us (2%)
  starting transfers between devices  10.3 us (2%)
  other arithmetic  6.69 us (1%)
    all_gather x2, waiting for transfers between devices, project_in(): lax.all_gather(stacked, FS, axis=1, tiled=True)  274 us
    all_gather x4, waiting for transfers between devices, stacked_from(): blocks = lax.all_gather(blocks, axes[k])  146 us
    all_to_all x2, blocking collectives, summed_on_arrival(): lax.all_to_all(blocks, axis, split_axis=0, concat_axis=0, tiled=True)  49.5 us
    dot_general x2, matrix products, project_in(): jnp.einsum('td,kdc->ktc', gathered, lax.all_gather(stacked, FS, axis=1, t...  24.3 us
    all_gather x2, blocking collectives, stacked_from(): blocks = lax.all_gather(blocks, axes[k])  12.6 us
  transfers between devices with their start and end apart: 8, of which 6 were waited for; matrix products, arithmetic and copies ran while one was open for 6% of the time, Pallas kernels for 0%

commit v1 on v0

v1 whole, which is shorter than its diff:
```python
import functools
import heapq

import jax
import jax.numpy as jnp
from jax import lax
from jax.experimental import pallas as pl
from jax.experimental.pallas import tpu as pltpu
from jax.sharding import Mesh
from jax.sharding import PartitionSpec as P

FS = ("fs_0", "fs_1", "fs_2")
REP_FS_TP = ("rep", "fs_0", "fs_1", "fs_2", "tp")
MESH = pl.DeviceIdType.MESH
BF16, F32 = jnp.bfloat16, jnp.float32

D = 2048
T = 640
H = 320
WIDTHS = (3072, 1024, 2816, 1408)
LINK = 46.0e3
LATENCY = 2.6
BACKLOG = 7.0

ALL = ("all",)
ME = ("rel", 0)


def half(k):
    return ("half", k)


def rel(k):
    return ("rel", k)


class Send:
    def __init__(self, stage, quarter, way, at, needs, rank, pieces):
        self.stage, self.quarter, self.way, self.at = stage, quarter, way, at
        self.needs, self.rank = needs, rank
        self.time = pieces * 16 * WIDTHS[stage] * 2 / LINK


def sends_of(stage):
    out = []

    def add(quarter, way, at, needs, rank, pieces):
        send = Send(stage, quarter, way, {"z": ME, "y": ME, "x": ME} | at, needs, rank, pieces)
        out.append(send)
        return send

    for quarter, (first, second) in enumerate((("x", "y"), ("y", "x"), ("x", "y"), ("y", "x"))):
        forth, back = first + "+", first + "-"
        plus = add(quarter, forth, {}, [], 0, 1)
        minus = add(quarter, back, {}, [], 0, 1)
        if quarter % 4 < 2:
            on = add(quarter, forth, {first: rel(-1)}, [plus], 1, 1)
        else:
            on = add(quarter, back, {first: rel(1)}, [minus], 1, 1)
        line = [plus, minus, on]
        forth, back = second + "+", second + "-"
        if quarter < 2:
            pa = add(quarter, forth, {first: half(0)}, line, 2, 2)
            pb = add(quarter, forth, {first: half(1)}, line, 3, 2)
            ma = add(quarter, back, {first: half(1)}, line, 2, 2)
            mb = add(quarter, back, {first: half(0)}, line, 3, 2)
            po = add(quarter, forth, {first: half(0), second: rel(-1)}, [pa], 4, 2)
            mo = add(quarter, back, {first: half(1), second: rel(1)}, [ma], 4, 2)
            add(quarter, "z+", {first: ALL}, line, 5, 4)
            add(quarter, "z+", {first: ALL, second: rel(-1)}, [pa, pb], 6, 4)
            add(quarter, "z-", {first: ALL, second: rel(1)}, [ma, mb], 6, 4)
            add(quarter, "z-", {first: ALL, second: rel(2)}, [po, mo], 7, 4)
        else:
            zp = add(quarter, "z+", {first: half(0)}, line, 2, 2)
            zm = add(quarter, "z-", {first: half(1)}, line, 2, 2)
            here, there = {first: ALL}, {first: ALL, "z": rel(1)}
            ph = add(quarter, forth, here, line, 3, 4)
            add(quarter, back, here, line, 3, 4)
            add(quarter, forth, there, [zp, zm], 4, 4)
            mt = add(quarter, back, there, [zp, zm], 4, 4)
            add(quarter, forth, here | {second: rel(-1)}, [ph], 5, 4)
            add(quarter, back, there | {second: rel(1)}, [mt], 5, 4)
    return out


def work_list():
    work = [("norm", 0, 4.0, None)]
    work += [("mix", j, 3.2, 0) for j in range(4)]
    work += [("out", j, 1.7, 1) for j in range(2)]
    work += [("again", 0, 5.0, None)]
    work += [("hide", j, 2.5, 2) for j in range(4)]
    return work


def plan():
    sends = [send for stage in range(4) for send in sends_of(stage)]
    waiting = sorted(range(len(sends)), key=lambda i: (sends[i].stage, sends[i].rank))
    number = {id(send): i for i, send in enumerate(sends)}
    left = [sum(send.stage == stage for send in sends) for stage in range(4)]
    free, arrived, flying, steps, now = {}, set(), [], [], 0.0
    work = work_list()

    def top_up():
        for i in list(waiting):
            send = sends[i]
            if free.get(send.way, 0.0) - now > BACKLOG:
                continue
            if all(number[id(need)] in arrived for need in send.needs):
                begin = max(free.get(send.way, 0.0), now)
                free[send.way] = begin + send.time
                heapq.heappush(flying, (free[send.way] + LATENCY, i))
                steps.append(("start", i))
                waiting.remove(i)

    top_up()
    while flying or work:
        while flying and flying[0][0] <= now:
            i = heapq.heappop(flying)[1]
            arrived.add(i)
            left[sends[i].stage] -= 1
            steps.append(("wait", i))
            top_up()
        if work and (work[0][3] is None or left[work[0][3]] == 0):
            name, j, time, _ = work.pop(0)
            steps.append((name, j))
            now += time
        elif flying:
            now = max(now, flying[0][0])
    return sends, steps, now


def region(send, place):
    at = []
    for dim, extent in (("z", 2), ("y", 4), ("x", 4)):
        how = send.at[dim]
        if how == ALL:
            at.append(pl.ds(0, extent))
        elif how[0] == "half":
            at.append(pl.ds(2 * how[1], 2))
        else:
            at.append(pl.ds(lax.rem(place[dim] + how[1] + extent, extent), 1))
    return (*at, pl.ds(16 * send.quarter, 16), pl.ds(0, WIDTHS[send.stage]))


def kernel(
    tokens, gain_one, w_b, w_c, w_v, taps, w_mix, gain_two, w_g, w_u, w_d, out,
    s0, s1, s2, s3, raw, normed, gated, part, came, came_two, resid, hidden, result,
    gain_v, taps_v, gain_two_v, acc_b, acc_c,
    local_sem, send_sem, recv_sem, pair_send, pair_recv,
):
    sends, steps, _ = plan()
    buffers = (s0, s1, s2, s3)
    rep, zl, y, x, tp = (lax.axis_index(name) for name in REP_FS_TP)
    me = {"z": zl, "y": y, "x": x}
    z = rep * 2 + zl

    def device(way):
        step = 1 if way[1] == "+" else 3
        if way[0] == "x":
            return (rep, zl, y, lax.rem(x + step, 4), tp)
        if way[0] == "y":
            return (rep, zl, lax.rem(y + step, 4), x, tp)
        there = lax.rem(z + step, 4)
        return (there // 2, lax.rem(there, 2), y, x, tp)

    partner = (rep, zl, y, x, 1 - tp)
    mine = pl.ds(pl.multiple_of(tp * H, H), H)
    other = pl.ds(pl.multiple_of((1 - tp) * H, H), H)

    def local(k, src, dst):
        return pltpu.make_async_copy(src, dst, local_sem.at[k])

    def slot(buffer, lo, n):
        return buffer.at[zl, y, x, pl.ds(0, 64), pl.ds(lo, n)]

    locals_ = [
        local(0, w_b, slot(s0, 0, 1024)),
        local(1, w_c, slot(s0, 1024, 1024)),
        local(2, w_v, slot(s0, 2048, 1024)),
        local(3, w_mix, slot(s1, 0, 1024)),
        local(4, w_g, slot(s2, 0, 1408)),
        local(5, w_u, slot(s2, 1408, 1408)),
        local(6, w_d, slot(s3, 0, 1408)),
        local(7, tokens, raw.at[mine, :]),
        local(8, gain_one, gain_v),
        local(9, taps, taps_v),
        local(10, gain_two, gain_two_v),
    ]
    ready_of = ((0, 1, 2), (3,), (4, 5), (6,))
    for copy in locals_:
        copy.start()

    barrier = pltpu.get_barrier_semaphore()
    greeted = [device(way) for way in ("x+", "x-", "y+", "y-", "z+", "z-")] + [partner]
    for peer in greeted:
        pl.semaphore_signal(barrier, inc=1, device_id=peer, device_id_type=MESH)
    pl.semaphore_wait(barrier, len(greeted))

    def to_partner(k, src, dst):
        return pltpu.make_async_remote_copy(
            src_ref=src, dst_ref=dst, send_sem=pair_send.at[k], recv_sem=pair_recv.at[k],
            device_id=partner, device_id_type=MESH,
        )

    def tokens_out():
        return to_partner(0, tokens, raw.at[mine, :])

    def tokens_in():
        return to_partner(0, tokens, raw.at[other, :])

    tokens_out().start()

    def outgoing(i):
        send = sends[i]
        where = buffers[send.stage].at[region(send, me)]
        return pltpu.make_async_remote_copy(
            src_ref=where, dst_ref=where, send_sem=send_sem.at[i], recv_sem=recv_sem.at[i],
            device_id=device(send.way), device_id_type=MESH,
        )

    def incoming(i):
        send = sends[i]
        back = send.way[0]
        place = dict(me)
        extent = 2 if back == "z" else 4
        place[back] = lax.rem(me[back] + (extent - 1 if send.way[1] == "+" else 1), extent)
        where = buffers[send.stage].at[region(send, place)]
        return pltpu.make_async_remote_copy(
            src_ref=where, dst_ref=where, send_sem=send_sem.at[i], recv_sem=recv_sem.at[i],
            device_id=device(send.way), device_id_type=MESH,
        )

    def scaled(values, gain):
        factor = lax.rsqrt(jnp.mean(values * values, axis=-1, keepdims=True) + 1e-06)
        return (values * factor * gain).astype(BF16)

    def norm(_):
        locals_[7].wait()
        locals_[8].wait()
        tokens_in().wait_recv()
        gain = gain_v[...]

        def chunk(r, carry):
            rows = pl.ds(pl.multiple_of(r * 32, 32), 32)
            normed[rows, :] = scaled(raw[rows, :].astype(F32), gain)
            return carry

        lax.fori_loop(0, T // 32, chunk, 0)

    def mix(j):
        if j == 0:
            locals_[9].wait()

        def columns(k):
            return s0[:, :, :, :, pl.ds(1024 * k + 256 * j, 256)].reshape(D, 256)

        def dot(k):
            return jnp.dot(normed[...], columns(k), preferred_element_type=F32).astype(BF16)

        acc_b[...] = dot(0)
        acc_c[...] = dot(1)
        mixed = acc_c[...].astype(F32) * dot(2).astype(F32)
        row = lax.broadcasted_iota(jnp.int32, (T, 256), 0)
        one = jnp.where(row >= 1, pltpu.roll(mixed, 1, 0), 0.0)
        two = jnp.where(row >= 2, pltpu.roll(mixed, 2, 0), 0.0)
        lanes = pl.ds(pl.multiple_of(tp * 1024 + 256 * j, 256), 256)
        tap = [taps_v[pl.ds(k, 1), lanes] for k in range(3)]
        convolved = tap[0] * two + tap[1] * one + tap[2] * mixed
        gated[:, pl.ds(256 * j, 256)] = (acc_b[...].astype(F32) * convolved).astype(BF16)

    def block(left, right):
        return lax.dot_general(
            left, right, (((1,), (1,)), ((), ())), preferred_element_type=F32
        ).astype(BF16)

    def part_out(j):
        cols = pl.ds(1024 * j, 1024)
        return to_partner(1 + j, part.at[:, cols], came.at[:, cols])

    def out_proj(j):
        def one(k, carry):
            cols = pl.ds(pl.multiple_of(1024 * j + 256 * k, 256), 256)
            part[:, cols] = block(gated[...], s1[j, k].reshape(256, 1024))
            return carry

        lax.fori_loop(0, 4, one, 0)
        part_out(j).start()

    def again(_):
        locals_[10].wait()
        part_out(0).wait_recv()
        part_out(1).wait_recv()
        gain = gain_two_v[...]

        def total(rows):
            sums = part[rows, :].astype(F32) + came[rows, :].astype(F32)
            return raw[rows, :].astype(F32) + sums

        def own(r, carry):
            rows = pl.ds(pl.multiple_of(tp * H + r * 32, 32), 32)
            values = total(rows)
            resid[pl.ds(pl.multiple_of(r * 32, 32), 32), :] = values
            normed[rows, :] = scaled(values, gain)
            return carry

        def others(r, carry):
            rows = pl.ds(pl.multiple_of((1 - tp) * H + r * 32, 32), 32)
            normed[rows, :] = scaled(total(rows), gain)
            return carry

        lax.fori_loop(0, H // 32, own, 0)
        lax.fori_loop(0, H // 32, others, 0)

    def hide(j):
        lo, n = ((0, 2), (2, 3), (5, 3), (8, 3))[j]

        def one(k, carry):
            at = pl.multiple_of(128 * (lo + k), 128)
            w_gate = s2[:, :, :, :, pl.ds(at, 128)].reshape(D, 128)
            w_up = s2[:, :, :, :, pl.ds(pl.multiple_of(at + 1408, 128), 128)].reshape(D, 128)
            both = jnp.dot(
                normed[...], jnp.concatenate([w_gate, w_up], axis=1), preferred_element_type=F32
            )
            gate, up = both[:, :128], both[:, 128:]
            hidden[:, pl.ds(at, 128)] = (gate / (1.0 + jnp.exp(-gate)) * up).astype(BF16)
            return carry

        lax.fori_loop(0, n, one, 0)

    act = {"norm": norm, "mix": mix, "out": out_proj, "again": again, "hide": hide}
    landed = set()
    for what, i in steps:
        if what == "start":
            stage = sends[i].stage
            if stage not in landed:
                landed.add(stage)
                for k in ready_of[stage]:
                    locals_[k].wait()
            outgoing(i).start()
        elif what == "wait":
            incoming(i).wait_recv()
        else:
            act[what](i)

    part_out(0).wait_send()
    part_out(1).wait_send()

    def down_out(k):
        cols = pl.ds(256 * k, 256)
        return to_partner(3 + k, part.at[other, cols], came_two.at[:, cols])

    for k in range(8):
        cols = pl.ds(256 * k, 256)
        part[:, cols] = block(hidden[...], s3[k // 4, k % 4].reshape(256, 1408))
        down_out(k).start()
    for k in range(8):
        cols = pl.ds(256 * k, 256)
        down_out(k).wait_recv()
        sums = part[mine, cols].astype(F32) + came_two[:, cols].astype(F32)
        result[:, cols] = (resid[:, cols] + 0.5 * sums).astype(BF16)
    done = local(0, result, out)
    done.start()
    for i in range(len(sends)):
        outgoing(i).wait_send()
    tokens_out().wait_send()
    for k in range(8):
        down_out(k).wait_send()
    done.wait()


def on_device(
    tokens, mix_gain, w_bgate, w_cgate, w_value, conv_taps, w_mixout, mlp_gain, w_gate, w_up, w_down
):
    count = len(plan()[0])
    anywhere = pl.BlockSpec(memory_space=pl.ANY)
    return pl.pallas_call(
        kernel,
        name="residual_block",
        out_shape=jax.ShapeDtypeStruct((H, D), BF16),
        in_specs=[anywhere] * 11,
        out_specs=anywhere,
        scratch_shapes=[
            *[pltpu.VMEM((2, 4, 4, 64, width), BF16) for width in WIDTHS],
            pltpu.VMEM((T, D), BF16),
            pltpu.VMEM((T, D), BF16),
            pltpu.VMEM((T, 1024), BF16),
            pltpu.VMEM((T, D), BF16),
            pltpu.VMEM((T, D), BF16),
            pltpu.VMEM((H, D), BF16),
            pltpu.VMEM((H, D), F32),
            pltpu.VMEM((T, 1408), BF16),
            pltpu.VMEM((H, D), BF16),
            pltpu.VMEM((1, D), F32),
            pltpu.VMEM((3, D), F32),
            pltpu.VMEM((1, D), F32),
            pltpu.VMEM((T, 256), BF16),
            pltpu.VMEM((T, 256), BF16),
            pltpu.SemaphoreType.DMA((11,)),
            pltpu.SemaphoreType.DMA((count,)),
            pltpu.SemaphoreType.DMA((count,)),
            pltpu.SemaphoreType.DMA((11,)),
            pltpu.SemaphoreType.DMA((11,)),
        ],
        compiler_params=pltpu.CompilerParams(
            collective_id=0, has_side_effects=True, vmem_limit_bytes=67043328
        ),
    )(
        tokens, mix_gain[None], w_bgate, w_cgate, w_value, conv_taps, w_mixout.T,
        mlp_gain[None], w_gate, w_up, w_down.T,
    )


def solution(mesh):
    finer = Mesh(
        mesh.devices.reshape(mesh.shape["rep"], 2, 4, 4, mesh.shape["tp"]),
        ("rep", "fs_0", "fs_1", "fs_2", "tp"),
    )
    return jax.shard_map(
        on_device,
        mesh=finer,
        in_specs=(
            P(REP_FS_TP, None),
            P(),
            P(FS, "tp"),
            P(FS, "tp"),
            P(FS, "tp"),
            P(),
            P("tp", FS),
            P(),
            P(FS, "tp"),
            P(FS, "tp"),
            P("tp", FS),
        ),
        out_specs=P(REP_FS_TP, None),
        check_vma=False,
    )
```

time: 568 us -> 156 us (0.27)
  waiting for transfers between devices: 420 us -> 0 us
  Pallas kernels: 0 us -> 154 us
  blocking collectives: 62.1 us -> 0 us
  matrix products: 34.9 us -> 0 us
  local copies, waits for them, and re-layouts: 20.1 us -> 2.52 us
  between operations: 13.6 us -> 0.01 us
  starting transfers between devices: 10.3 us -> 0 us
  other arithmetic: 6.69 us -> 0 us
    all_gather x6 -> x0, waiting for transfers between devices: 420 us -> none  [the longest x2 274 us: project_in(): lax.all_gather(stacked, FS, axis=1, tiled=True)]
    pallas_call x0 -> x1, Pallas kernels: none -> 154 us  [on_device(): pl.pallas_call(kernel, name='residual_block', out_shape=jax.ShapeDtypeStr...]
    all_to_all x2 -> x0, blocking collectives: 49.5 us -> none  [summed_on_arrival(): lax.all_to_all(blocks, axis, split_axis=0, concat_axis=0, tiled=True)]
    dot_general x4 -> x0, matrix products: 34.9 us -> none  [the longest x2 24.3 us: project_in(): jnp.einsum('td,kdc->ktc', gathered, lax.all_gather(stacked, FS, axis=1, t...]
    all_gather x2 -> x0, blocking collectives: 12.6 us -> none  [stacked_from(): blocks = lax.all_gather(blocks, axes[k])]
    transpose x2 -> x0, local copies, waits for them, and re-layouts: 10.6 us -> none  [stacked_from(): blocks = blocks.transpose(*back, *range(len(axes), blocks.ndim))]
    all_to_all x2 -> x0, starting transfers between devices: 10.1 us -> none  [sent_to_all(): lax.all_to_all(jnp.broadcast_to(array[None], (peers, *array.shape)), axis...]
  transfers between devices with their start and end apart: 8 -> 0, of which waited for: 6 -> 0; matrix products, arithmetic and copies ran while one was open for 6% -> 0% of each run, Pallas kernels for 0% -> 0%
where the time goes in v1:
time: 156 us
  Pallas kernels  154 us (99%)
  local copies, waits for them, and re-layouts  2.52 us (2%)
    pallas_call x1, Pallas kernels, on_device(): pl.pallas_call(kernel, name='residual_block', out_shape=jax.ShapeDtypeStr...  154 us

profile of v1, /device:TPU:1, one launch (start us, length us, event | category | flops | bytes accessed | tf_op | source)
XLA Modules:
  0.0 156.3 jit_solution(11589889432225076170)
XLA Ops:
  0.0 153.8 %residual_block.1 = bf16[320,2048]{1,0:T(8,128)(2,1)} custom-call(bf16[320,2048]{1,0:T(8,128)(2,1)} %tokens.1, f32[1,2048]{1,0:T(1,128)} %bitcast.6, bf16[64,1024]{1,0:T(8,128)(2,1)} %w_b.1, bf16[64,1024]{1,0:T(8,128)(2,1)} %w_c.1, bf16[64,1024]{1,0:T(8,128)(2,1)} %w_v.1, f32[3,2048]{1,0:T(4,128)} %taps.1, bf16[64,1024]{1,0:T(8,128)(2,1)} %bitcast.5, ...), custom_call_target="tpu_custom_call" | custom-call | tf_op jit(solution)/shard_map/residual_block/pallas_call | solution.py:376
  153.8 2.5 %copy.13 = bf16[320,2048]{1,0:T(8,128)(2,1)} copy(bf16[320,2048]{1,0:T(8,128)(2,1)} %residual_block.1) | data formatting | bytes 2621440

commit v2 on v1

--- a/solution.py
+++ b/solution.py
@@ -18,7 +18,7 @@
 T = 640
 H = 320
 WIDTHS = (3072, 1024, 2816, 1408)
-LINK = 46.0e3
+LINK = 45.6e3
 LATENCY = 2.6
 BACKLOG = 7.0
 
@@ -66,10 +66,14 @@
             mb = add(quarter, back, {first: half(0)}, line, 3, 2)
             po = add(quarter, forth, {first: half(0), second: rel(-1)}, [pa], 4, 2)
             mo = add(quarter, back, {first: half(1), second: rel(1)}, [ma], 4, 2)
-            add(quarter, "z+", {first: ALL}, line, 5, 4)
-            add(quarter, "z+", {first: ALL, second: rel(-1)}, [pa, pb], 6, 4)
-            add(quarter, "z-", {first: ALL, second: rel(1)}, [ma, mb], 6, 4)
-            add(quarter, "z-", {first: ALL, second: rel(2)}, [po, mo], 7, 4)
+            up, down = ("z+", "z-") if quarter == 0 else ("z-", "z+")
+            add(quarter, up, {}, [], 0, 1)
+            add(quarter, up, {first: rel(-1)}, [plus], 2, 1)
+            add(quarter, up, {first: rel(1)}, [minus], 2, 1)
+            add(quarter, up, {first: rel(2)}, [on], 2, 1)
+            add(quarter, up, {first: ALL, second: rel(-1)}, [pa, pb], 6, 4)
+            add(quarter, down, {first: ALL, second: rel(1)}, [ma, mb], 6, 4)
+            add(quarter, down, {first: ALL, second: rel(2)}, [po, mo], 7, 4)
         else:
             zp = add(quarter, "z+", {first: half(0)}, line, 2, 2)
             zm = add(quarter, "z-", {first: half(1)}, line, 2, 2)
@@ -83,12 +87,17 @@
     return out
 
 
+def near(send):
+    return (send.way[0] == "z") == (send.at["z"] != ME)
+
+
 def work_list():
     work = [("norm", 0, 4.0, None)]
     work += [("mix", j, 3.2, 0) for j in range(4)]
     work += [("out", j, 1.7, 1) for j in range(2)]
     work += [("again", 0, 5.0, None)]
     work += [("hide", j, 2.5, 2) for j in range(4)]
+    work += [("down", 0, 3.0, 4), ("down", 1, 3.0, 3)]
     return work
 
 
@@ -97,6 +106,7 @@
     waiting = sorted(range(len(sends)), key=lambda i: (sends[i].stage, sends[i].rank))
     number = {id(send): i for i, send in enumerate(sends)}
     left = [sum(send.stage == stage for send in sends) for stage in range(4)]
+    left.append(sum(send.stage == 3 and near(send) for send in sends))
     free, arrived, flying, steps, now = {}, set(), [], [], 0.0
     work = work_list()
 
@@ -118,6 +128,7 @@
             i = heapq.heappop(flying)[1]
             arrived.add(i)
             left[sends[i].stage] -= 1
+            left[4] -= sends[i].stage == 3 and near(sends[i])
             steps.append(("wait", i))
             top_up()
         if work and (work[0][3] is None or left[work[0][3]] == 0):
@@ -143,8 +154,8 @@
 
 
 def kernel(
-    tokens, gain_one, w_b, w_c, w_v, taps, w_mix, gain_two, w_g, w_u, w_d, out,
-    s0, s1, s2, s3, raw, normed, gated, part, came, came_two, resid, hidden, result,
+    tokens, gain_one, w_b, w_c, w_v, taps, w_mix, gain_two, w_g, w_u, w_d, total, came_two,
+    s0, s1, s2, s3, raw, normed, gated, part, came, resid, hidden,
     gain_v, taps_v, gain_two_v, acc_b, acc_c,
     local_sem, send_sem, recv_sem, pair_send, pair_recv,
 ):
@@ -292,20 +303,20 @@
         part_out(1).wait_recv()
         gain = gain_two_v[...]
 
-        def total(rows):
+        def joined(rows):
             sums = part[rows, :].astype(F32) + came[rows, :].astype(F32)
             return raw[rows, :].astype(F32) + sums
 
         def own(r, carry):
             rows = pl.ds(pl.multiple_of(tp * H + r * 32, 32), 32)
-            values = total(rows)
+            values = joined(rows)
             resid[pl.ds(pl.multiple_of(r * 32, 32), 32), :] = values
             normed[rows, :] = scaled(values, gain)
             return carry
 
         def others(r, carry):
             rows = pl.ds(pl.multiple_of((1 - tp) * H + r * 32, 32), 32)
-            normed[rows, :] = scaled(total(rows), gain)
+            normed[rows, :] = scaled(joined(rows), gain)
             return carry
 
         lax.fori_loop(0, H // 32, own, 0)
@@ -327,7 +338,40 @@
 
         lax.fori_loop(0, n, one, 0)
 
-    act = {"norm": norm, "mix": mix, "out": out_proj, "again": again, "hide": hide}
+    def half_of(j):
+        return pl.ds(pl.multiple_of(1024 * lax.rem(zl + j, 2), 1024), 1024)
+
+    def down_out(j):
+        cols = half_of(j)
+        return to_partner(3 + j, part.at[other, cols], came_two.at[:, cols])
+
+    def down_home(j):
+        cols = half_of(j)
+        return local(j, resid.at[:, cols], total.at[:, cols])
+
+    def down(j):
+        plane = lax.rem(zl + j, 2)
+        if j == 0:
+            part_out(0).wait_send()
+            part_out(1).wait_send()
+
+        def theirs(k, carry):
+            cols = pl.ds(pl.multiple_of(1024 * plane + 256 * k, 256), 256)
+            part[other, cols] = block(hidden[other, :], s3[plane, k].reshape(256, 1408))
+            return carry
+
+        def ours(k, carry):
+            cols = pl.ds(pl.multiple_of(1024 * plane + 256 * k, 256), 256)
+            own = block(hidden[mine, :], s3[plane, k].reshape(256, 1408))
+            resid[:, cols] = resid[:, cols] + 0.5 * own.astype(F32)
+            return carry
+
+        lax.fori_loop(0, 4, theirs, 0)
+        down_out(j).start()
+        lax.fori_loop(0, 4, ours, 0)
+        down_home(j).start()
+
+    act = {"norm": norm, "mix": mix, "out": out_proj, "again": again, "hide": hide, "down": down}
     landed = set()
     for what, i in steps:
         if what == "start":
@@ -342,30 +386,12 @@
         else:
             act[what](i)
 
-    part_out(0).wait_send()
-    part_out(1).wait_send()
-
-    def down_out(k):
-        cols = pl.ds(256 * k, 256)
-        return to_partner(3 + k, part.at[other, cols], came_two.at[:, cols])
-
-    for k in range(8):
-        cols = pl.ds(256 * k, 256)
-        part[:, cols] = block(hidden[...], s3[k // 4, k % 4].reshape(256, 1408))
-        down_out(k).start()
-    for k in range(8):
-        cols = pl.ds(256 * k, 256)
-        down_out(k).wait_recv()
-        sums = part[mine, cols].astype(F32) + came_two[:, cols].astype(F32)
-        result[:, cols] = (resid[:, cols] + 0.5 * sums).astype(BF16)
-    done = local(0, result, out)
-    done.start()
     for i in range(len(sends)):
         outgoing(i).wait_send()
     tokens_out().wait_send()
-    for k in range(8):
-        down_out(k).wait_send()
-    done.wait()
+    for j in range(2):
+        down_out(j).wait()
+        down_home(j).wait()
 
 
 def on_device(
@@ -373,12 +399,12 @@
 ):
     count = len(plan()[0])
     anywhere = pl.BlockSpec(memory_space=pl.ANY)
-    return pl.pallas_call(
+    total, came = pl.pallas_call(
         kernel,
         name="residual_block",
-        out_shape=jax.ShapeDtypeStruct((H, D), BF16),
+        out_shape=(jax.ShapeDtypeStruct((H, D), F32), jax.ShapeDtypeStruct((H, D), BF16)),
         in_specs=[anywhere] * 11,
-        out_specs=anywhere,
+        out_specs=(anywhere, anywhere),
         scratch_shapes=[
             *[pltpu.VMEM((2, 4, 4, 64, width), BF16) for width in WIDTHS],
             pltpu.VMEM((T, D), BF16),
@@ -386,10 +412,8 @@
             pltpu.VMEM((T, 1024), BF16),
             pltpu.VMEM((T, D), BF16),
             pltpu.VMEM((T, D), BF16),
-            pltpu.VMEM((H, D), BF16),
             pltpu.VMEM((H, D), F32),
             pltpu.VMEM((T, 1408), BF16),
-            pltpu.VMEM((H, D), BF16),
             pltpu.VMEM((1, D), F32),
             pltpu.VMEM((3, D), F32),
             pltpu.VMEM((1, D), F32),
@@ -398,8 +422,8 @@
             pltpu.SemaphoreType.DMA((11,)),
             pltpu.SemaphoreType.DMA((count,)),
             pltpu.SemaphoreType.DMA((count,)),
-            pltpu.SemaphoreType.DMA((11,)),
-            pltpu.SemaphoreType.DMA((11,)),
+            pltpu.SemaphoreType.DMA((5,)),
+            pltpu.SemaphoreType.DMA((5,)),
         ],
         compiler_params=pltpu.CompilerParams(
             collective_id=0, has_side_effects=True, vmem_limit_bytes=67043328
@@ -408,6 +432,7 @@
         tokens, mix_gain[None], w_bgate, w_cgate, w_value, conv_taps, w_mixout.T,
         mlp_gain[None], w_gate, w_up, w_down.T,
     )
+    return (total + 0.5 * came.astype(F32)).astype(BF16)
 
 
 def solution(mesh):

time: 156 us -> 147 us (0.942)
  Pallas kernels: 154 us -> 143 us
  other arithmetic: 0 us -> 3.58 us
  local copies, waits for them, and re-layouts: 2.52 us -> 0 us
    pallas_call x1, Pallas kernels: 154 us -> 143 us  [on_device(): pl.pallas_call(kernel, name='residual_block', out_shape=(jax.ShapeDtypeSt...]
    convert_element_type x0 -> x1, other arithmetic: none -> 3.58 us  [on_device(): return (total + 0.5 * came.astype(F32)).astype(BF16)]
    unnamed x1 -> x0, local copies, waits for them, and re-layouts: 2.52 us -> none
where the time goes in v2:
time: 147 us
  Pallas kernels  143 us (97%)
  other arithmetic  3.58 us (2%)
    pallas_call x1, Pallas kernels, on_device(): pl.pallas_call(kernel, name='residual_block', out_shape=(jax.ShapeDtypeSt...  143 us
    convert_element_type x1, other arithmetic, on_device(): return (total + 0.5 * came.astype(F32)).astype(BF16)  3.58 us

profile of v2, /device:TPU:1, one launch (start us, length us, event | category | flops | bytes accessed | tf_op | source)
XLA Modules:
  0.0 146.8 jit_solution(8315384353692234311)
XLA Ops:
  0.0 143.2 %residual_block.1 = (f32[320,2048]{1,0:T(8,128)}, bf16[320,2048]{1,0:T(8,128)(2,1)}) custom-call(bf16[320,2048]{1,0:T(8,128)(2,1)} %tokens.1, f32[1,2048]{1,0:T(1,128)} %bitcast.6, bf16[64,1024]{1,0:T(8,128)(2,1)} %w_b.1, bf16[64,1024]{1,0:T(8,128)(2,1)} %w_c.1, bf16[64,1024]{1,0:T(8,128)(2,1)} %w_v.1, f32[3,2048]{1,0:T(4,128)} %taps.1, ...), custom_call_target="tpu_custom_call" | custom-call | tf_op jit(solution)/shard_map/residual_block/pallas_call | solution.py:402
  143.2 3.6 %add_convert_fusion = bf16[320,2048]{1,0:T(8,128)(2,1)} fusion(f32[320,2048]{1,0:T(8,128)} %get-tuple-element.7, bf16[320,2048]{1,0:T(8,128)(2,1)} %get-tuple-element.8), kind=kLoop, calls=%fused_computation | loop fusion | flops 2621440 | bytes 5242880 | tf_op jit(solution)/shard_map/convert_element_type | solution.py:435

commit v3 on v2

v3 whole, which is shorter than its diff:
```python
import heapq

import jax
import jax.numpy as jnp
from jax import lax
from jax.experimental import pallas as pl
from jax.experimental.pallas import tpu as pltpu
from jax.sharding import Mesh
from jax.sharding import PartitionSpec as P

FS = ("fs_0", "fs_1", "fs_2")
REP_FS_TP = ("rep", "fs_0", "fs_1", "fs_2", "tp")
MESH = pl.DeviceIdType.MESH
BF16, F32 = jnp.bfloat16, jnp.float32

D = 2048
T = 640
H = 320
WIDTHS = (1536, 512, 2816, 1408)
LINK = 45.6e3
PAIR = 500.0e3
LATENCY = 2.6
PAIR_LATENCY = 1.5
BACKLOG = 2.7
HOLD = 0.0

RANKS = (
    -2, -2, -2, -2, -3, -4, -4, -4, -4, -4, -4, -4, -4, -4, -4, 1260, 1396, 1285, 1398, 1398,
    1232, 1347, 1278, 1292, 1311, 1343, 1281, 1343, 1379, 1237, 1376, 1398, 1253, 1336, 1303,
    1369, 1303, 1303, 1399, 1450, 1576, 1304, 1198, 1344, 1339, 1499, 1282, 1303, 1303, 1369,
    1303, 1375, 1376, 1220, 1336, 1398, 1472, 1253, 1209, 1376, 1209, 1328, 1376, 1313, 1216,
    1278, 1290, 1347, 1293, 1434, 1298, 1390, 1390, 1548, 1549, 1487, 1492, 1419, 1426, 1419,
    1365, 1514, 1499, 1465, 1489, 1482, 1387, 1460, 1387, 1515, 1415, 1388, 1365, 1443, 1354,
    1546, 1445, 1430, 1516, 1359, 1459, 1340, 1415, 1371, 1415, 1511, 1443, 1482, 1482, 1483,
    1598, 1467, 1384, 1267, 1415, 1415, 1441, 1482, 1533, 1468, 1423, 1451, 1431, 1449, 1482,
    1495, 1632, 1593, 1676, 1683, 1656, 1652, 1650, 1639, 1683, 1738, 1929, 1809, 1925, 1802,
    1736, 1521, 1624, 1632, 1625, 1739, 1727, 1714, 1739, 1739, 1895, 1780, 1888, 1842, 1802,
    1802, 1979, 1613, 1556, 1716, 1694, 1620, 1733, 1657, 1874, 2006, 1860, 1673, 1969, 1738,
    1613, 1568, 1613, 1703, 1733, 1599, 1657, 1732, 1925, 1722, 1701, 1802, 1714, 1555, 1667,
    1565, 1706, 1496, 1628, 1674, 1674, 1674, 2096, 2040, 2015, 2140, 2008, 1937, 2205, 1621,
    1534, 1591, 1704, 1698, 1684, 1674, 1737, 1733, 1908, 2057, 2037, 2096, 2008, 2034, 2008,
    1563, 1504, 1635, 1978, 1941, 1843, 1958, 1654, 1655, 1953, 1886, 1644, 2008, 1721, 1545,
    1632, 1853, 1910, 1911, 1939, 1673, 1721, 2008, 1945, 1703, 2008,
)

ALL = ("all",)
ME = ("rel", 0)


def half(k):
    return ("half", k)


def rel(k):
    return ("rel", k)


class Send:
    def __init__(self, kind, way, needs, rank, size, stage=None, quarter=None, at=None, index=None):
        self.kind, self.way, self.needs, self.rank = kind, way, needs, rank
        self.stage, self.quarter, self.at, self.index = stage, quarter, at, index
        self.time = size / (PAIR if way == "pair" else LINK)
        self.latency = PAIR_LATENCY if way == "pair" else LATENCY


def all_sends():
    out = []

    def add(quarter, way, at, needs, rank, pieces):
        at = {"z": ME, "y": ME, "x": ME} | at
        size = pieces * 16 * WIDTHS[stage] * 2
        send = Send("part", way, list(needs), rank, size, stage, quarter, at)
        out.append(send)
        return send

    def other(kind, way, needs, rank, size, index, stage=None):
        send = Send(kind, way, list(needs), rank, size, stage, None, None, index)
        out.append(send)
        return send

    row = D * 2
    for p in range(2):
        token = other("token", "zw", [], -2, 160 * row, p)
        other("relay", "pair", [token], -2, 160 * row, p)
    other("swap", "pair", [], -3, H * row, 0)
    for j in range(2):
        other("mate", "pair", [("mate", j)], -4, H * 1024 * 2, j)
        other("sum", "zw", [("sum", j)], -4, 160 * row, j)
        other("home", "pair", [("home", j)], -4, H * 1024 * 2, j)
        other("again", "pair", [("again", j)], -4, 160 * row, j)
        other("down", "pair", [("down", 2 * j)], -4, H * 1024 * 2, j)

    for stage in range(2):
        base = 10 * stage
        orders = (("x", "y"), ("x", "y"), ("y", "x"), ("y", "x") if stage == 0 else ("x", "y"))
        for quarter, (first, second) in enumerate(orders):
            if quarter == 3:
                over = [add(quarter, "zd", {}, [], base, 1)]
                for far in range(2):
                    z = {"z": rel(far)}
                    start = over if far else []
                    plus = add(quarter, first + "+", z, start, base + far, 1)
                    minus = add(quarter, first + "-", z, start, base + far, 1)
                    if far:
                        on = add(quarter, first + "-", z | {first: rel(1)}, [minus], base + 2, 1)
                    else:
                        on = add(quarter, first + "+", z | {first: rel(-1)}, [plus], base + 2, 1)
                    line = [plus, minus, on] + start
                    z = z | {first: ALL}
                    plus = add(quarter, second + "+", z, line, base + 3, 4)
                    minus = add(quarter, second + "-", z, line, base + 3, 4)
                    if far:
                        add(quarter, second + "-", z | {second: rel(1)}, [minus], base + 4, 4)
                    else:
                        add(quarter, second + "+", z | {second: rel(-1)}, [plus], base + 4, 4)
                continue
            forth, back = first + "+", first + "-"
            plus = add(quarter, forth, {}, [], base, 1)
            minus = add(quarter, back, {}, [], base, 1)
            if quarter == 1:
                on = add(quarter, back, {first: rel(1)}, [minus], base + 1, 1)
            else:
                on = add(quarter, forth, {first: rel(-1)}, [plus], base + 1, 1)
            line = [plus, minus, on]
            over = [
                add(quarter, "zd", {first: rel(k)}, needs, base + 1, 1)
                for k, needs in ((0, []), (-1, [plus]), (1, [minus]), (2, [on]))
            ]
            forth, back = second + "+", second + "-"
            if quarter == 0:
                pa = add(quarter, forth, {first: half(0)}, line, base + 2, 2)
                pb = add(quarter, forth, {first: half(1)}, line, base + 3, 2)
                ma = add(quarter, back, {first: half(1)}, line, base + 2, 2)
                mb = add(quarter, back, {first: half(0)}, line, base + 3, 2)
                po = add(quarter, forth, {first: half(0), second: rel(-1)}, [pa], base + 4, 2)
                mo = add(quarter, back, {first: half(1), second: rel(1)}, [ma], base + 4, 2)
                add(quarter, "zd", {first: ALL, second: rel(-1)}, [pa, pb], base + 5, 4)
                add(quarter, "zd", {first: ALL, second: rel(1)}, [ma, mb], base + 5, 4)
                add(quarter, "zd", {first: ALL, second: rel(2)}, [po, mo], base + 6, 4)
            else:
                here, there = {first: ALL}, {first: ALL, "z": rel(1)}
                ph = add(quarter, forth, here, line, base + 3, 4)
                add(quarter, back, here, line, base + 3, 4)
                add(quarter, forth, there, over, base + 4, 4)
                mt = add(quarter, back, there, over, base + 4, 4)
                add(quarter, forth, here | {second: rel(-1)}, [ph], base + 5, 4)
                add(quarter, back, there | {second: rel(1)}, [mt], base + 5, 4)
    orders = (("x", "y"), ("y", "x"), ("x", "y"), ("y", "x"))
    for stage in range(2, 4):
        base = 20 + 10 * (stage - 2)
        early = 14 + 8 * (stage - 2)
        for quarter, (first, second) in enumerate(orders):
            forth, back = first + "+", first + "-"
            plus = add(quarter, forth, {}, [], early, 1)
            minus = add(quarter, back, {}, [], early, 1)
            if quarter < 2:
                on = add(quarter, forth, {first: rel(-1)}, [plus], early, 1)
            else:
                on = add(quarter, back, {first: rel(1)}, [minus], early, 1)
            line = [plus, minus, on]
            forth, back = second + "+", second + "-"
            if quarter < 2:
                pa = add(quarter, forth, {first: half(0)}, line, base + 2, 2)
                pb = add(quarter, forth, {first: half(1)}, line, base + 3, 2)
                ma = add(quarter, back, {first: half(1)}, line, base + 2, 2)
                mb = add(quarter, back, {first: half(0)}, line, base + 3, 2)
                po = add(quarter, forth, {first: half(0), second: rel(-1)}, [pa], base + 4, 2)
                mo = add(quarter, back, {first: half(1), second: rel(1)}, [ma], base + 4, 2)
                add(quarter, "zw", {}, [], early, 1)
                add(quarter, "zw", {first: rel(-1)}, [plus], early, 1)
                add(quarter, "zw", {first: rel(1)}, [minus], early, 1)
                add(quarter, "zw", {first: rel(2)}, [on], early, 1)
                add(quarter, "zd", {first: ALL, second: rel(-1)}, [pa, pb], base + 5, 4)
                add(quarter, "zd", {first: ALL, second: rel(1)}, [ma, mb], base + 5, 4)
                add(quarter, "zw", {first: ALL, second: rel(2)}, [po, mo], base + 6, 4)
            else:
                over = [
                    add(quarter, "zd", {first: rel(k)}, needs, base + 2, 1)
                    for k, needs in ((0, []), (-1, [plus]), (1, [minus]), (2, [on]))
                ]
                here, there = {first: ALL}, {first: ALL, "z": rel(1)}
                ph = add(quarter, forth, here, line, base + 3, 4)
                add(quarter, back, here, line, base + 3, 4)
                add(quarter, forth, there, over, base + 4, 4)
                mt = add(quarter, back, there, over, base + 4, 4)
                add(quarter, forth, here | {second: rel(-1)}, [ph], base + 5, 4)
                add(quarter, back, there | {second: rel(1)}, [mt], base + 5, 4)
    return out


def near(send):
    return (send.way[0] == "z") == (send.at["z"] != ME)


def work_list(sends):
    def kind(name, *index):
        return [s for s in sends if s.kind == name and (not index or s.index in index)]

    def stage(k):
        return [s for s in sends if s.stage == k]

    last = stage(3)
    out = [("norm", k, 1.0, kind("swap")) for k in range(4)]
    out += [("norm", k, 1.0, kind("token") + kind("relay")) for k in range(4, 8)]
    out += [("mix", k, 1.6 if k % 3 == 2 else 0.8, stage(0)) for k in range(6)]
    out += [("mate", k, 1.0, stage(1)) for k in range(2)]
    out += [("sum", k, 0.7, kind("mate")) for k in range(2)]
    out += [("mix", k, 1.6 if k % 3 == 2 else 0.8, []) for k in range(6, 12)]
    out += [("home", k, 1.0, []) for k in range(2)]
    out += [("again", k, 1.4, kind("home") + kind("sum", k)) for k in range(2)]
    out += [("hide", k, 0.95, kind("again") + stage(2)) for k in range(11)]
    out += [("down", k, 1.5, [s for s in last if near(s)]) for k in range(2)]
    out += [("down", k, 1.5, last) for k in range(2, 4)]
    return out


def plan(ranks=RANKS):
    sends = all_sends()
    if ranks:
        for send, rank in zip(sends, ranks, strict=True):
            send.rank = rank
    work = work_list(sends)
    number = {id(send): i for i, send in enumerate(sends)}
    followers, missing = {}, []
    for i, send in enumerate(sends):
        missing.append(len(send.needs))
        for need in send.needs:
            key = need if isinstance(need, tuple) else number[id(need)]
            followers.setdefault(key, []).append(i)
    ready = {send.way: [] for send in sends}
    free = dict.fromkeys(ready, 0.0)
    got, flying, steps, held, now = set(), [], [], [], 0.0

    def release(i):
        if sends[i].kind == "part" and sends[i].stage > 1 and now < HOLD:
            held.append(i)
        else:
            heapq.heappush(ready[sends[i].way], (sends[i].rank, i))

    def arrive(key):
        got.add(key)
        for i in followers.get(key, ()):
            missing[i] -= 1
            if missing[i] == 0:
                release(i)

    def top_up():
        if now >= HOLD:
            while held:
                release(held.pop())
        for way, queue in ready.items():
            while queue and (queue[0][0] < 0 or free[way] - now <= BACKLOG):
                i = heapq.heappop(queue)[1]
                free[way] = max(free[way], now) + sends[i].time
                heapq.heappush(flying, (free[way] + sends[i].latency, i))
                steps.append(("start", i))

    for i, count in enumerate(missing):
        if count == 0:
            release(i)
    top_up()
    step = 0
    needs = [[number[id(need)] for need in piece[3]] for piece in work]
    while flying or step < len(work):
        while flying and flying[0][0] <= now:
            i = heapq.heappop(flying)[1]
            steps.append(("wait", i))
            arrive(i)
            top_up()
        if step < len(work) and got.issuperset(needs[step]):
            name, j, time, _ = work[step]
            step += 1
            steps.append((name, j))
            now += time
            arrive((name, j))
            top_up()
        elif flying:
            now = max(now, flying[0][0])
    return sends, steps, now


def region(send, place):
    at = []
    for dim, extent in (("z", 2), ("y", 4), ("x", 4)):
        how = send.at[dim]
        if how == ALL:
            at.append(pl.ds(0, extent))
        elif how[0] == "half":
            at.append(pl.ds(2 * how[1], 2))
        else:
            at.append(pl.ds(lax.rem(place[dim] + how[1] + extent, extent), 1))
    return (*at, pl.ds(16 * send.quarter, 16), pl.ds(0, WIDTHS[send.stage]))


def kernel(
    tokens, gain_one, w_b, w_c, w_v, taps, w_mix, gain_two, w_g, w_u, w_d, total, came_two,
    s0, s1, s2, s3, raw, normed, gated, to_mate, from_mate, summed, mate_sum, to_home, from_home,
    resid, hidden, gain_v, taps_v, gain_two_v, acc_b, acc_c, local_sem, send_sem, recv_sem,
):
    sends, steps, _ = plan()
    buffers = (s0, s1, s2, s3)
    rep, zl, y, x, tp = (lax.axis_index(name) for name in REP_FS_TP)
    me = {"z": zl, "y": y, "x": x}

    def device(way):
        if way == "pair":
            return (rep, zl, y, x, 1 - tp)
        if way == "zd":
            return (rep, 1 - zl, y, x, tp)
        if way == "zw":
            return (1 - rep, 1 - zl, y, x, tp)
        step = 1 if way[1] == "+" else 3
        if way[0] == "x":
            return (rep, zl, y, lax.rem(x + step, 4), tp)
        return (rep, zl, lax.rem(y + step, 4), x, tp)

    def rows_of(core, start=0, n=H):
        return pl.ds(pl.multiple_of(core * H + start, 32), n)

    mine, other = rows_of(tp), rows_of(1 - tp)

    def local(k, src, dst):
        return pltpu.make_async_copy(src, dst, local_sem.at[k])

    def slot(buffer, lo, n):
        return buffer.at[zl, y, x, pl.ds(0, 64), pl.ds(lo, n)]

    def share(weight):
        return weight.at[:, pl.ds(pl.multiple_of(rep * 512, 512), 512)]

    locals_ = [
        local(0, share(w_b), slot(s0, 0, 512)),
        local(1, share(w_c), slot(s0, 512, 512)),
        local(2, share(w_v), slot(s0, 1024, 512)),
        local(3, share(w_mix), slot(s1, 0, 512)),
        local(4, w_g, slot(s2, 0, 1408)),
        local(5, w_u, slot(s2, 1408, 1408)),
        local(6, w_d, slot(s3, 0, 1408)),
        local(7, tokens, raw.at[0, mine, :]),
        local(8, gain_one, gain_v),
        local(9, taps, taps_v),
        local(10, gain_two, gain_two_v),
    ]
    ready_of = ((0, 1, 2), (3,), (4, 5), (6,))
    for copy in locals_:
        copy.start()

    barrier = pltpu.get_barrier_semaphore()
    ways = ("x+", "x-", "y+", "y-", "zd", "zw", "pair")
    for way in ways:
        pl.semaphore_signal(barrier, inc=1, device_id=device(way), device_id_type=MESH)
    pl.semaphore_wait(barrier, len(ways))

    def ends(send, place, core):
        j = send.index
        cols = None if j is None else pl.ds(1024 * (j % 2), 1024)
        if send.kind == "part":
            where = buffers[send.stage].at[region(send, place)]
            return where, where
        if send.kind == "token":
            return tokens.at[pl.ds(160 * j, 160), :], raw.at[1, rows_of(core, 160 * j, 160), :]
        if send.kind == "relay":
            where = raw.at[1, rows_of(core, 160 * j, 160), :]
            return where, where
        if send.kind == "swap":
            return tokens, raw.at[0, rows_of(core), :]
        if send.kind == "mate":
            return to_mate.at[:, cols], from_mate.at[:, cols]
        if send.kind == "sum":
            rows = pl.ds(160 * j, 160)
            return summed.at[rows, :], mate_sum.at[rows, :]
        if send.kind == "home":
            return to_home.at[:, cols], from_home.at[:, cols]
        if send.kind == "again":
            where = normed.at[0, rows_of(core, 160 * j, 160), :]
            return where, where
        lanes = half_of(j, place["z"])
        return to_mate.at[:, lanes], came_two.at[:, lanes]

    def half_of(j, z):
        return pl.ds(pl.multiple_of(1024 * lax.rem(z + j, 2), 1024), 1024)

    def copy_of(i, place, core):
        src, dst = ends(sends[i], place, core)
        return pltpu.make_async_remote_copy(
            src_ref=src, dst_ref=dst, send_sem=send_sem.at[i], recv_sem=recv_sem.at[i],
            device_id=device(sends[i].way), device_id_type=MESH,
        )

    def outgoing(i):
        return copy_of(i, me, tp)

    def incoming(i):
        way, place = sends[i].way, dict(me)
        if way in ("zd", "zw"):
            place["z"] = 1 - zl
        elif way != "pair":
            place[way[0]] = lax.rem(me[way[0]] + (3 if way[1] == "+" else 1), 4)
        return copy_of(i, place, 1 - tp if way == "pair" else tp)

    def scaled(values, gain):
        factor = lax.rsqrt(jnp.mean(values * values, axis=-1, keepdims=True) + 1e-06)
        return (values * factor * gain).astype(BF16)

    def norm(step):
        c, part = step // 4, step % 4
        if step == 0:
            locals_[7].wait()
            locals_[8].wait()
        gain = gain_v[...]

        def chunk(r, carry):
            rows = pl.ds(pl.multiple_of(r * 32, 32), 32)
            normed[c, rows, :] = scaled(raw[c, rows, :].astype(F32), gain)
            return carry

        lax.fori_loop(5 * part, 5 * part + 5, chunk, 0)

    def mix(step):
        c, j, k = 1 - step // 6, step // 3 % 2, step % 3
        if step == 0:
            locals_[9].wait()

        def dot(k):
            w = s0[:, :, :, :, pl.ds(512 * k + 256 * j, 256)].reshape(D, 256)
            return jnp.dot(normed[c], w, preferred_element_type=F32).astype(BF16)

        if k < 2:
            (acc_b, acc_c)[k][...] = dot(k)
            return
        mixed = acc_c[...].astype(F32) * dot(2).astype(F32)
        row = lax.broadcasted_iota(jnp.int32, (T, 256), 0)
        one = jnp.where(row >= 1, pltpu.roll(mixed, 1, 0), 0.0)
        two = jnp.where(row >= 2, pltpu.roll(mixed, 2, 0), 0.0)
        lanes = pl.ds(pl.multiple_of(tp * 1024 + rep * 512 + 256 * j, 256), 256)
        tap = [taps_v[pl.ds(k, 1), lanes] for k in range(3)]
        convolved = tap[0] * two + tap[1] * one + tap[2] * mixed
        gated[c, :, pl.ds(256 * j, 256)] = (acc_b[...].astype(F32) * convolved).astype(BF16)

    def block(left, right):
        return lax.dot_general(left, right, (((1,), (1,)), ((), ())), preferred_element_type=F32)

    def product(c, j, away):
        def one(k, carry):
            cols = pl.ds(pl.multiple_of(1024 * j + 256 * k, 256), 256)
            w = s1[j, k].reshape(256, 512)
            away[:, cols] = block(gated[c, other, :], w).astype(BF16)
            resid[:, cols] = block(gated[c, mine, :], w)
            return carry

        lax.fori_loop(0, 4, one, 0)

    def mate(j):
        product(1, j, to_mate)

    def home(j):
        product(0, j, to_home)

    def add_up(p):
        def chunk(r, carry):
            rows = pl.ds(pl.multiple_of(160 * p + r * 32, 32), 32)
            summed[rows, :] = (resid[rows, :] + from_mate[rows, :].astype(F32)).astype(BF16)
            return carry

        lax.fori_loop(0, 5, chunk, 0)

    def again(p):
        if p == 0:
            locals_[10].wait()
        gain = gain_two_v[...]

        def chunk(r, carry):
            rows = pl.ds(pl.multiple_of(160 * p + r * 32, 32), 32)
            here = pl.ds(pl.multiple_of(tp * H + 160 * p + r * 32, 32), 32)
            sums = resid[rows, :] + from_home[rows, :].astype(F32)
            sums = sums + mate_sum[rows, :].astype(F32)
            values = raw[0, here, :].astype(F32) + sums
            resid[rows, :] = values
            normed[0, here, :] = scaled(values, gain)
            return carry

        lax.fori_loop(0, 5, chunk, 0)

    def hide(k):
        w_gate = s2[:, :, :, :, pl.ds(128 * k, 128)].reshape(D, 128)
        w_up = s2[:, :, :, :, pl.ds(1408 + 128 * k, 128)].reshape(D, 128)
        both = jnp.dot(
            normed[0], jnp.concatenate([w_gate, w_up], axis=1), preferred_element_type=F32
        )
        gate, up = both[:, :128], both[:, 128:]
        hidden[:, pl.ds(128 * k, 128)] = (gate / (1.0 + jnp.exp(-gate)) * up).astype(BF16)

    def down_home(j):
        cols = half_of(j, zl)
        return local(j, resid.at[:, cols], total.at[:, cols])

    def down(step):
        j = step // 2
        plane = lax.rem(zl + j, 2)

        def theirs(k, carry):
            cols = pl.ds(pl.multiple_of(1024 * plane + 256 * k, 256), 256)
            w = s3[plane, k].reshape(256, 1408)
            to_mate[:, cols] = block(hidden[other, :], w).astype(BF16)
            return carry

        def ours(k, carry):
            cols = pl.ds(pl.multiple_of(1024 * plane + 256 * k, 256), 256)
            own = block(hidden[mine, :], s3[plane, k].reshape(256, 1408)).astype(BF16)
            resid[:, cols] = resid[:, cols] + 0.5 * own.astype(F32)
            return carry

        if step == 0:
            for i, send in enumerate(sends):
                if send.kind == "mate":
                    outgoing(i).wait_send()
        if step % 2 == 0:
            lax.fori_loop(0, 4, theirs, 0)
        else:
            lax.fori_loop(0, 4, ours, 0)
            down_home(j).start()

    act = {
        "norm": norm, "mix": mix, "mate": mate, "sum": add_up, "home": home, "again": again,
        "hide": hide, "down": down,
    }
    landed = set()
    for what, i in steps:
        if what == "start":
            send = sends[i]
            if send.kind == "part" and send.stage not in landed:
                landed.add(send.stage)
                for k in ready_of[send.stage]:
                    locals_[k].wait()
            outgoing(i).start()
        elif what == "wait":
            incoming(i).wait_recv()
        else:
            act[what](i)

    for i, send in enumerate(sends):
        if send.kind != "mate":
            outgoing(i).wait_send()
    for j in range(2):
        down_home(j).wait()


def on_device(
    tokens, mix_gain, w_bgate, w_cgate, w_value, conv_taps, w_mixout, mlp_gain, w_gate, w_up, w_down
):
    count = len(all_sends())
    anywhere = pl.BlockSpec(memory_space=pl.ANY)
    total, came = pl.pallas_call(
        kernel,
        name="residual_block",
        out_shape=(jax.ShapeDtypeStruct((H, D), F32), jax.ShapeDtypeStruct((H, D), BF16)),
        in_specs=[anywhere] * 11,
        out_specs=(anywhere, anywhere),
        scratch_shapes=[
            *[pltpu.VMEM((2, 4, 4, 64, width), BF16) for width in WIDTHS],
            pltpu.VMEM((2, T, D), BF16),
            pltpu.VMEM((2, T, D), BF16),
            pltpu.VMEM((2, T, 512), BF16),
            *[pltpu.VMEM((H, D), BF16)] * 6,
            pltpu.VMEM((H, D), F32),
            pltpu.VMEM((T, 1408), BF16),
            pltpu.VMEM((1, D), F32),
            pltpu.VMEM((3, D), F32),
            pltpu.VMEM((1, D), F32),
            pltpu.VMEM((T, 256), BF16),
            pltpu.VMEM((T, 256), BF16),
            pltpu.SemaphoreType.DMA((11,)),
            pltpu.SemaphoreType.DMA((count,)),
            pltpu.SemaphoreType.DMA((count,)),
        ],
        compiler_params=pltpu.CompilerParams(
            collective_id=0, has_side_effects=True, vmem_limit_bytes=67043328
        ),
    )(
        tokens, mix_gain[None], w_bgate, w_cgate, w_value, conv_taps, w_mixout.T,
        mlp_gain[None], w_gate, w_up, w_down.T,
    )
    return (total + 0.5 * came.astype(F32)).astype(BF16)


def solution(mesh):
    finer = Mesh(
        mesh.devices.reshape(mesh.shape["rep"], 2, 4, 4, mesh.shape["tp"]),
        ("rep", "fs_0", "fs_1", "fs_2", "tp"),
    )
    return jax.shard_map(
        on_device,
        mesh=finer,
        in_specs=(
            P(REP_FS_TP, None),
            P(),
            P(FS, "tp"),
            P(FS, "tp"),
            P(FS, "tp"),
            P(),
            P("tp", FS),
            P(),
            P(FS, "tp"),
            P(FS, "tp"),
            P("tp", FS),
        ),
        out_specs=P(REP_FS_TP, None),
        check_vma=False,
    )
```

time: 147 us -> 137 us (0.932)
  Pallas kernels: 143 us -> 133 us
    pallas_call x1, Pallas kernels: 143 us -> 133 us  [on_device(): pl.pallas_call(kernel, name='residual_block', out_shape=(jax.ShapeDtypeSt...]
where the time goes in v3:
time: 137 us
  Pallas kernels  133 us (97%)
  other arithmetic  3.58 us (3%)
    pallas_call x1, Pallas kernels, on_device(): pl.pallas_call(kernel, name='residual_block', out_shape=(jax.ShapeDtypeSt...  133 us
    convert_element_type x1, other arithmetic, on_device(): return (total + 0.5 * came.astype(F32)).astype(BF16)  3.58 us

profile of v3, /device:TPU:1, one launch (start us, length us, event | category | flops | bytes accessed | tf_op | source)
XLA Modules:
  0.0 136.8 jit_solution(6221070723546158410)
XLA Ops:
  0.0 133.2 %residual_block.1 = (f32[320,2048]{1,0:T(8,128)}, bf16[320,2048]{1,0:T(8,128)(2,1)}) custom-call(bf16[320,2048]{1,0:T(8,128)(2,1)} %tokens.1, f32[1,2048]{1,0:T(1,128)} %bitcast.6, bf16[64,1024]{1,0:T(8,128)(2,1)} %w_b.1, bf16[64,1024]{1,0:T(8,128)(2,1)} %w_c.1, bf16[64,1024]{1,0:T(8,128)(2,1)} %w_v.1, f32[3,2048]{1,0:T(4,128)} %taps.1, ...), custom_call_target="tpu_custom_call" | custom-call | tf_op jit(solution)/shard_map/residual_block/pallas_call | solution.py:553
  133.2 3.6 %add_convert_fusion = bf16[320,2048]{1,0:T(8,128)(2,1)} fusion(f32[320,2048]{1,0:T(8,128)} %get-tuple-element.7, bf16[320,2048]{1,0:T(8,128)(2,1)} %get-tuple-element.8), kind=kLoop, calls=%fused_computation | loop fusion | flops 2621440 | bytes 5242880 | tf_op jit(solution)/shard_map/convert_element_type | solution.py:583

commit v4 on v3

--- a/solution.py
+++ b/solution.py
@@ -21,26 +21,23 @@
 PAIR = 500.0e3
 LATENCY = 2.6
 PAIR_LATENCY = 1.5
-BACKLOG = 2.7
+BACKLOG = 2.75
 HOLD = 0.0
 
 RANKS = (
-    -2, -2, -2, -2, -3, -4, -4, -4, -4, -4, -4, -4, -4, -4, -4, 1260, 1396, 1285, 1398, 1398,
-    1232, 1347, 1278, 1292, 1311, 1343, 1281, 1343, 1379, 1237, 1376, 1398, 1253, 1336, 1303,
-    1369, 1303, 1303, 1399, 1450, 1576, 1304, 1198, 1344, 1339, 1499, 1282, 1303, 1303, 1369,
-    1303, 1375, 1376, 1220, 1336, 1398, 1472, 1253, 1209, 1376, 1209, 1328, 1376, 1313, 1216,
-    1278, 1290, 1347, 1293, 1434, 1298, 1390, 1390, 1548, 1549, 1487, 1492, 1419, 1426, 1419,
-    1365, 1514, 1499, 1465, 1489, 1482, 1387, 1460, 1387, 1515, 1415, 1388, 1365, 1443, 1354,
-    1546, 1445, 1430, 1516, 1359, 1459, 1340, 1415, 1371, 1415, 1511, 1443, 1482, 1482, 1483,
-    1598, 1467, 1384, 1267, 1415, 1415, 1441, 1482, 1533, 1468, 1423, 1451, 1431, 1449, 1482,
-    1495, 1632, 1593, 1676, 1683, 1656, 1652, 1650, 1639, 1683, 1738, 1929, 1809, 1925, 1802,
-    1736, 1521, 1624, 1632, 1625, 1739, 1727, 1714, 1739, 1739, 1895, 1780, 1888, 1842, 1802,
-    1802, 1979, 1613, 1556, 1716, 1694, 1620, 1733, 1657, 1874, 2006, 1860, 1673, 1969, 1738,
-    1613, 1568, 1613, 1703, 1733, 1599, 1657, 1732, 1925, 1722, 1701, 1802, 1714, 1555, 1667,
-    1565, 1706, 1496, 1628, 1674, 1674, 1674, 2096, 2040, 2015, 2140, 2008, 1937, 2205, 1621,
-    1534, 1591, 1704, 1698, 1684, 1674, 1737, 1733, 1908, 2057, 2037, 2096, 2008, 2034, 2008,
-    1563, 1504, 1635, 1978, 1941, 1843, 1958, 1654, 1655, 1953, 1886, 1644, 2008, 1721, 1545,
-    1632, 1853, 1910, 1911, 1939, 1673, 1721, 2008, 1945, 1703, 2008,
+    -2, -2, -2, -2, -3, -4, -4, -4, -4, -4, -4, -4, -4, -4, -4, 492, 63, 454, 0, 290, 1432,
+    314, 34, 0, 0, 375, 150, 0, 28, 811, 150, 0, 393, 0, 573, 0, 0, 1361, 0, 40, 501, 262,
+    1309, 640, 915, 302, 0, 0, 356, 0, 0, 0, 106, 291, 0, 779, 0, 0, 0, 0, 0, 548, 0, 0, 468,
+    1054, 0, 0, 0, 51, 0, 0, 0, 0, 0, 0, 0, 0, 0, 0, 0, 0, 0, 0, 0, 0, 0, 0, 0, 0, 0, 0, 0, 0,
+    0, 621, 0, 0, 0, 0, 0, 309, 955, 0, 623, 0, 0, 0, 950, 0, 0, 0, 0, 0, 0, 0, 0, 0, 0, 0, 0,
+    0, 0, 1131, 281, 575, 1257, 1552, 1547, 1543, 1225, 776, 1418, 2204, 0, 2680, 2569, 1574,
+    887, 1925, 2595, 1362, 1412, 765, 1672, 1361, 2101, 1154, 2976, 2949, 2010, 2192, 2850,
+    932, 2246, 1875, 1502, 0, 1087, 698, 1318, 1578, 1679, 78, 2113, 2575, 1672, 2158, 2132,
+    1880, 0, 984, 2117, 1024, 825, 1075, 1235, 4064, 2301, 2442, 1256, 1700, 2357, 2885, 2992,
+    1410, 1175, 2161, 2291, 769, 2794, 2363, 1753, 2634, 3794, 1175, 1926, 359, 1316, 349,
+    2795, 675, 1848, 2322, 3078, 2550, 3003, 2491, 1092, 3045, 2981, 754, 925, 2185, 1422,
+    1621, 1290, 3485, 2508, 2327, 1968, 1531, 1439, 3130, 1946, 2190, 3375, 2217, 1064, 530,
+    3110, 1418, 3573, 2220, 1887, 1113, 1543, 1484,
 )
 
 ALL = ("all",)
@@ -159,7 +156,7 @@
                 on = add(quarter, back, {first: rel(1)}, [minus], early, 1)
             line = [plus, minus, on]
             forth, back = second + "+", second + "-"
-            if quarter < 2:
+            if quarter < 4 - stage:
                 pa = add(quarter, forth, {first: half(0)}, line, base + 2, 2)
                 pb = add(quarter, forth, {first: half(1)}, line, base + 3, 2)
                 ma = add(quarter, back, {first: half(1)}, line, base + 2, 2)
@@ -170,13 +167,16 @@
                 add(quarter, "zw", {first: rel(-1)}, [plus], early, 1)
                 add(quarter, "zw", {first: rel(1)}, [minus], early, 1)
                 add(quarter, "zw", {first: rel(2)}, [on], early, 1)
-                add(quarter, "zd", {first: ALL, second: rel(-1)}, [pa, pb], base + 5, 4)
+                late = "zw" if stage == 3 else "zd"
+                add(quarter, late, {first: ALL, second: rel(-1)}, [pa, pb], base + 5, 4)
                 add(quarter, "zd", {first: ALL, second: rel(1)}, [ma, mb], base + 5, 4)
-                add(quarter, "zw", {first: ALL, second: rel(2)}, [po, mo], base + 6, 4)
+                add(quarter, late, {first: ALL, second: rel(2)}, [po, mo], base + 6, 4)
             else:
                 over = [
-                    add(quarter, "zd", {first: rel(k)}, needs, base + 2, 1)
-                    for k, needs in ((0, []), (-1, [plus]), (1, [minus]), (2, [on]))
+                    add(quarter, way, {first: rel(k)}, needs, base + 2, 1)
+                    for way, k, needs in (
+                        ("zw", 0, []), ("zd", -1, [plus]), ("zd", 1, [minus]), ("zw", 2, [on])
+                    )
                 ]
                 here, there = {first: ALL}, {first: ALL, "z": rel(1)}
                 ph = add(quarter, forth, here, line, base + 3, 4)

time: 137 us -> 135 us (0.985)
    pallas_call x1, Pallas kernels: 133 us -> 132 us  [on_device(): pl.pallas_call(kernel, name='residual_block', out_shape=(jax.ShapeDtypeSt...]
where the time goes in v4:
time: 135 us
  Pallas kernels  132 us (98%)
  other arithmetic  3.58 us (3%)
    pallas_call x1, Pallas kernels, on_device(): pl.pallas_call(kernel, name='residual_block', out_shape=(jax.ShapeDtypeSt...  132 us
    convert_element_type x1, other arithmetic, on_device(): return (total + 0.5 * came.astype(F32)).astype(BF16)  3.58 us

profile of v4, /device:TPU:1, one launch (start us, length us, event | category | flops | bytes accessed | tf_op | source)
XLA Modules:
  0.0 135.2 jit_solution(8226695497528088732)
XLA Ops:
  0.0 131.6 %residual_block.1 = (f32[320,2048]{1,0:T(8,128)}, bf16[320,2048]{1,0:T(8,128)(2,1)}) custom-call(bf16[320,2048]{1,0:T(8,128)(2,1)} %tokens.1, f32[1,2048]{1,0:T(1,128)} %bitcast.6, bf16[64,1024]{1,0:T(8,128)(2,1)} %w_b.1, bf16[64,1024]{1,0:T(8,128)(2,1)} %w_c.1, bf16[64,1024]{1,0:T(8,128)(2,1)} %w_v.1, f32[3,2048]{1,0:T(4,128)} %taps.1, ...), custom_call_target="tpu_custom_call" | custom-call | tf_op jit(solution)/shard_map/residual_block/pallas_call | solution.py:553
  131.6 3.6 %add_convert_fusion = bf16[320,2048]{1,0:T(8,128)(2,1)} fusion(f32[320,2048]{1,0:T(8,128)} %get-tuple-element.7, bf16[320,2048]{1,0:T(8,128)(2,1)} %get-tuple-element.8), kind=kLoop, calls=%fused_computation | loop fusion | flops 2621440 | bytes 5242880 | tf_op jit(solution)/shard_map/convert_element_type | solution.py:583

commit v5 on v4

--- a/solution.py
+++ b/solution.py
@@ -21,23 +21,24 @@
 PAIR = 500.0e3
 LATENCY = 2.6
 PAIR_LATENCY = 1.5
-BACKLOG = 2.75
+BACKLOG = 3.63
 HOLD = 0.0
 
 RANKS = (
-    -2, -2, -2, -2, -3, -4, -4, -4, -4, -4, -4, -4, -4, -4, -4, 492, 63, 454, 0, 290, 1432,
-    314, 34, 0, 0, 375, 150, 0, 28, 811, 150, 0, 393, 0, 573, 0, 0, 1361, 0, 40, 501, 262,
-    1309, 640, 915, 302, 0, 0, 356, 0, 0, 0, 106, 291, 0, 779, 0, 0, 0, 0, 0, 548, 0, 0, 468,
-    1054, 0, 0, 0, 51, 0, 0, 0, 0, 0, 0, 0, 0, 0, 0, 0, 0, 0, 0, 0, 0, 0, 0, 0, 0, 0, 0, 0, 0,
-    0, 621, 0, 0, 0, 0, 0, 309, 955, 0, 623, 0, 0, 0, 950, 0, 0, 0, 0, 0, 0, 0, 0, 0, 0, 0, 0,
-    0, 0, 1131, 281, 575, 1257, 1552, 1547, 1543, 1225, 776, 1418, 2204, 0, 2680, 2569, 1574,
-    887, 1925, 2595, 1362, 1412, 765, 1672, 1361, 2101, 1154, 2976, 2949, 2010, 2192, 2850,
-    932, 2246, 1875, 1502, 0, 1087, 698, 1318, 1578, 1679, 78, 2113, 2575, 1672, 2158, 2132,
-    1880, 0, 984, 2117, 1024, 825, 1075, 1235, 4064, 2301, 2442, 1256, 1700, 2357, 2885, 2992,
-    1410, 1175, 2161, 2291, 769, 2794, 2363, 1753, 2634, 3794, 1175, 1926, 359, 1316, 349,
-    2795, 675, 1848, 2322, 3078, 2550, 3003, 2491, 1092, 3045, 2981, 754, 925, 2185, 1422,
-    1621, 1290, 3485, 2508, 2327, 1968, 1531, 1439, 3130, 1946, 2190, 3375, 2217, 1064, 530,
-    3110, 1418, 3573, 2220, 1887, 1113, 1543, 1484,
+    -2, -2, -2, -2, -3, -4, -4, -4, -4, -4, -4, -4, -4, -4, -4, 0, 0, 0, 0, 180, 0, 0, 0, 86,
+    610, 932, 0, 0, 253, 1060, 152, 152, 0, 0, 657, 0, 76, 66, 0, 1303, 0, 0, 0, 0, 0, 174, 0,
+    0, 1304, 0, 347, 0, 0, 38, 0, 0, 0, 0, 0, 0, 0, 0, 0, 0, 191, 0, 133, 0, 305, 142, 758,
+    1182, 976, 844, 1933, 1743, 2379, 382, 1059, 2039, 960, 383, 810, 501, 1142, 911, 159,
+    279, 0, 336, 1479, 508, 2417, 1070, 2346, 1253, 1178, 1180, 1781, 937, 543, 872, 36, 835,
+    619, 0, 409, 1297, 605, 1329, 1832, 599, 0, 0, 1089, 2275, 0, 0, 903, 0, 512, 301, 2029,
+    62, 733, 1508, 2212, 2892, 1842, 2040, 2501, 2127, 1964, 2098, 1464, 2393, 1730, 2390,
+    1605, 2886, 3497, 85, 1970, 2672, 2035, 2441, 2542, 1890, 3075, 1917, 3166, 1683, 1850,
+    1351, 2360, 2190, 2195, 2128, 1539, 2430, 2304, 1355, 2861, 3162, 2038, 2675, 1621, 2660,
+    2806, 2379, 2168, 1408, 1888, 645, 2875, 3370, 2129, 1855, 2554, 2152, 2733, 878, 2605,
+    3136, 2152, 2804, 2540, 2990, 2399, 4163, 2270, 2567, 2758, 4079, 2763, 3264, 4850, 3769,
+    2914, 3168, 3413, 3179, 3976, 3214, 3858, 2758, 3674, 2067, 4128, 4220, 3085, 4208, 2998,
+    1946, 3153, 3902, 3715, 3731, 4469, 3206, 4713, 3271, 4368, 4244, 4523, 2114, 2052, 2732,
+    3026, 3628, 2666, 1819, 2988, 3263, 4367, 2146, 2494, 3611,
 )
 
 ALL = ("all",)
@@ -146,6 +147,7 @@
     for stage in range(2, 4):
         base = 20 + 10 * (stage - 2)
         early = 14 + 8 * (stage - 2)
+        wrap = "zw" if stage == 2 else "zd"
         for quarter, (first, second) in enumerate(orders):
             forth, back = first + "+", first + "-"
             plus = add(quarter, forth, {}, [], early, 1)
@@ -167,15 +169,15 @@
                 add(quarter, "zw", {first: rel(-1)}, [plus], early, 1)
                 add(quarter, "zw", {first: rel(1)}, [minus], early, 1)
                 add(quarter, "zw", {first: rel(2)}, [on], early, 1)
-                late = "zw" if stage == 3 else "zd"
-                add(quarter, late, {first: ALL, second: rel(-1)}, [pa, pb], base + 5, 4)
+                soon = "zw" if stage == 2 and quarter == 0 else "zd"
+                add(quarter, soon, {first: ALL, second: rel(-1)}, [pa, pb], base + 5, 4)
                 add(quarter, "zd", {first: ALL, second: rel(1)}, [ma, mb], base + 5, 4)
-                add(quarter, late, {first: ALL, second: rel(2)}, [po, mo], base + 6, 4)
+                add(quarter, "zd", {first: ALL, second: rel(2)}, [po, mo], base + 6, 4)
             else:
                 over = [
                     add(quarter, way, {first: rel(k)}, needs, base + 2, 1)
                     for way, k, needs in (
-                        ("zw", 0, []), ("zd", -1, [plus]), ("zd", 1, [minus]), ("zw", 2, [on])
+                        (wrap, 0, []), (wrap, -1, [plus]), ("zd", 1, [minus]), (wrap, 2, [on])
                     )
                 ]
                 here, there = {first: ALL}, {first: ALL, "z": rel(1)}
@@ -202,13 +204,13 @@
     last = stage(3)
     out = [("norm", k, 1.0, kind("swap")) for k in range(4)]
     out += [("norm", k, 1.0, kind("token") + kind("relay")) for k in range(4, 8)]
-    out += [("mix", k, 1.6 if k % 3 == 2 else 0.8, stage(0)) for k in range(6)]
+    out += [("mix", k, 1.3 if k % 3 == 2 else 0.7, stage(0)) for k in range(6)]
     out += [("mate", k, 1.0, stage(1)) for k in range(2)]
     out += [("sum", k, 0.7, kind("mate")) for k in range(2)]
-    out += [("mix", k, 1.6 if k % 3 == 2 else 0.8, []) for k in range(6, 12)]
+    out += [("mix", k, 1.3 if k % 3 == 2 else 0.7, []) for k in range(6, 12)]
     out += [("home", k, 1.0, []) for k in range(2)]
     out += [("again", k, 1.4, kind("home") + kind("sum", k)) for k in range(2)]
-    out += [("hide", k, 0.95, kind("again") + stage(2)) for k in range(11)]
+    out += [("hide", k, 0.72, kind("again") + stage(2)) for k in range(11)]
     out += [("down", k, 1.5, [s for s in last if near(s)]) for k in range(2)]
     out += [("down", k, 1.5, last) for k in range(2, 4)]
     return out
@@ -276,7 +278,44 @@
             top_up()
         elif flying:
             now = max(now, flying[0][0])
-    return sends, steps, now
+    return sends, eager(sends, steps, work, number), now
+
+
+def eager(sends, steps, work, number):
+    queues, followed, pieces = {}, set(), {(piece[0], piece[1]): piece for piece in work}
+    for what, i in steps:
+        if what == "start":
+            queues.setdefault(sends[i].way, []).append(i)
+    needs = {}
+    for i, send in enumerate(sends):
+        needs[i] = [n if isinstance(n, tuple) else number[id(n)] for n in send.needs]
+        followed.update(needs[i])
+    out, got = [], set()
+
+    def start_all():
+        for queue in queues.values():
+            while queue and got.issuperset(needs[queue[0]]):
+                out.append(("start", queue.pop(0)))
+
+    def wait_for(i):
+        if i not in got:
+            got.add(i)
+            out.append(("wait", i))
+            start_all()
+
+    start_all()
+    for what, i in steps:
+        if what == "wait" and i in followed:
+            wait_for(i)
+        elif what not in ("start", "wait"):
+            for need in pieces[what, i][3]:
+                wait_for(number[id(need)])
+            out.append((what, i))
+            got.add((what, i))
+            start_all()
+    for i in range(len(sends)):
+        wait_for(i)
+    return out
 
 
 def region(send, place):
@@ -490,10 +529,6 @@
         gate, up = both[:, :128], both[:, 128:]
         hidden[:, pl.ds(128 * k, 128)] = (gate / (1.0 + jnp.exp(-gate)) * up).astype(BF16)
 
-    def down_home(j):
-        cols = half_of(j, zl)
-        return local(j, resid.at[:, cols], total.at[:, cols])
-
     def down(step):
         j = step // 2
         plane = lax.rem(zl + j, 2)
@@ -507,7 +542,7 @@
         def ours(k, carry):
             cols = pl.ds(pl.multiple_of(1024 * plane + 256 * k, 256), 256)
             own = block(hidden[mine, :], s3[plane, k].reshape(256, 1408)).astype(BF16)
-            resid[:, cols] = resid[:, cols] + 0.5 * own.astype(F32)
+            total[:, cols] = resid[:, cols] + 0.5 * own.astype(F32)
             return carry
 
         if step == 0:
@@ -518,7 +553,6 @@
             lax.fori_loop(0, 4, theirs, 0)
         else:
             lax.fori_loop(0, 4, ours, 0)
-            down_home(j).start()
 
     act = {
         "norm": norm, "mix": mix, "mate": mate, "sum": add_up, "home": home, "again": again,
@@ -541,8 +575,6 @@
     for i, send in enumerate(sends):
         if send.kind != "mate":
             outgoing(i).wait_send()
-    for j in range(2):
-        down_home(j).wait()
 
 
 def on_device(
@@ -553,9 +585,9 @@
     total, came = pl.pallas_call(
         kernel,
         name="residual_block",
-        out_shape=(jax.ShapeDtypeStruct((H, D), F32), jax.ShapeDtypeStruct((H, D), BF16)),
+        out_shape=(pltpu.VMEM((H, D), F32), pltpu.VMEM((H, D), BF16)),
         in_specs=[anywhere] * 11,
-        out_specs=(anywhere, anywhere),
+        out_specs=(pl.BlockSpec(memory_space=pltpu.VMEM),) * 2,
         scratch_shapes=[
             *[pltpu.VMEM((2, 4, 4, 64, width), BF16) for width in WIDTHS],
             pltpu.VMEM((2, T, D), BF16),
@@ -574,7 +606,7 @@
             pltpu.SemaphoreType.DMA((count,)),
         ],
         compiler_params=pltpu.CompilerParams(
-            collective_id=0, has_side_effects=True, vmem_limit_bytes=67043328
+            collective_id=0, has_side_effects=True, vmem_limit_bytes=60 * 2**20
         ),
     )(
         tokens, mix_gain[None], w_bgate, w_cgate, w_value, conv_taps, w_mixout.T,

time: 135 us -> 125 us (0.926)
  Pallas kernels: 132 us -> 124 us
  other arithmetic: 3.58 us -> 1.48 us
    pallas_call x1, Pallas kernels: 132 us -> 124 us  [on_device(): pl.pallas_call(kernel, name='residual_block', out_shape=(pltpu.VMEM((H, D...]
    convert_element_type x1, other arithmetic: 3.58 us -> 1.48 us  [on_device(): return (total + 0.5 * came.astype(F32)).astype(BF16)]
where the time goes in v5:
time: 125 us
  Pallas kernels  124 us (99%)
  other arithmetic  1.48 us (1%)
    pallas_call x1, Pallas kernels, on_device(): pl.pallas_call(kernel, name='residual_block', out_shape=(pltpu.VMEM((H, D...  124 us

profile of v5, /device:TPU:1, one launch (start us, length us, event | category | flops | bytes accessed | tf_op | source)
XLA Modules:
  0.0 125.2 jit_solution(11448806489721575318)
XLA Ops:
  0.0 123.7 %residual_block.1 = (f32[320,2048]{1,0:T(8,128)S(1)}, bf16[320,2048]{1,0:T(8,128)(2,1)S(1)}) custom-call(bf16[320,2048]{1,0:T(8,128)(2,1)} %tokens.1, f32[1,2048]{1,0:T(1,128)} %bitcast.6, bf16[64,1024]{1,0:T(8,128)(2,1)} %w_b.1, bf16[64,1024]{1,0:T(8,128)(2,1)} %w_c.1, bf16[64,1024]{1,0:T(8,128)(2,1)} %w_v.1, f32[3,2048]{1,0:T(4,128)} %taps.1, ...), custom_call_target="tpu_custom_call" | custom-call | tf_op jit(solution)/shard_map/residual_block/pallas_call | solution.py:585
  123.7 1.5 %add_convert_fusion = bf16[320,2048]{1,0:T(8,128)(2,1)} fusion(f32[320,2048]{1,0:T(8,128)S(1)} %get-tuple-element.7, bf16[320,2048]{1,0:T(8,128)(2,1)S(1)} %get-tuple-element.8), kind=kLoop, calls=%fused_computation | loop fusion | flops 2621440 | bytes 5242880 | tf_op jit(solution)/shard_map/convert_element_type | solution.py:615

commit v6 on v5

--- a/solution.py
+++ b/solution.py
@@ -17,28 +17,30 @@
 T = 640
 H = 320
 WIDTHS = (1536, 512, 2816, 1408)
-LINK = 45.6e3
+LINK = 45.1e3
 PAIR = 500.0e3
-LATENCY = 2.6
-PAIR_LATENCY = 1.5
-BACKLOG = 3.63
+LATENCY = 3.4
+PAIR_LATENCY = 1.8
+BACKLOG = 2.93
 HOLD = 0.0
 
 RANKS = (
-    -2, -2, -2, -2, -3, -4, -4, -4, -4, -4, -4, -4, -4, -4, -4, 0, 0, 0, 0, 180, 0, 0, 0, 86,
-    610, 932, 0, 0, 253, 1060, 152, 152, 0, 0, 657, 0, 76, 66, 0, 1303, 0, 0, 0, 0, 0, 174, 0,
-    0, 1304, 0, 347, 0, 0, 38, 0, 0, 0, 0, 0, 0, 0, 0, 0, 0, 191, 0, 133, 0, 305, 142, 758,
-    1182, 976, 844, 1933, 1743, 2379, 382, 1059, 2039, 960, 383, 810, 501, 1142, 911, 159,
-    279, 0, 336, 1479, 508, 2417, 1070, 2346, 1253, 1178, 1180, 1781, 937, 543, 872, 36, 835,
-    619, 0, 409, 1297, 605, 1329, 1832, 599, 0, 0, 1089, 2275, 0, 0, 903, 0, 512, 301, 2029,
-    62, 733, 1508, 2212, 2892, 1842, 2040, 2501, 2127, 1964, 2098, 1464, 2393, 1730, 2390,
-    1605, 2886, 3497, 85, 1970, 2672, 2035, 2441, 2542, 1890, 3075, 1917, 3166, 1683, 1850,
-    1351, 2360, 2190, 2195, 2128, 1539, 2430, 2304, 1355, 2861, 3162, 2038, 2675, 1621, 2660,
-    2806, 2379, 2168, 1408, 1888, 645, 2875, 3370, 2129, 1855, 2554, 2152, 2733, 878, 2605,
-    3136, 2152, 2804, 2540, 2990, 2399, 4163, 2270, 2567, 2758, 4079, 2763, 3264, 4850, 3769,
-    2914, 3168, 3413, 3179, 3976, 3214, 3858, 2758, 3674, 2067, 4128, 4220, 3085, 4208, 2998,
-    1946, 3153, 3902, 3715, 3731, 4469, 3206, 4713, 3271, 4368, 4244, 4523, 2114, 2052, 2732,
-    3026, 3628, 2666, 1819, 2988, 3263, 4367, 2146, 2494, 3611,
+    -2, -2, -2, -2, -3, -4, -4, -4, -4, -4, -4, -4, -4, -4, -4, 1002, 1057, 1057, 1292, 1292,
+    1292, 1292, 1113, 1182, 1113, 1182, 1182, 1182, 1252, 1252, 1252, 1198, 988, 946, 1100,
+    1100, 1100, 1140, 1155, 1252, 1252, 1155, 1252, 1246, 988, 1044, 1044, 1100, 1100, 1100,
+    1075, 1155, 1252, 1252, 1155, 1272, 1405, 988, 1044, 1100, 1100, 1155, 1138, 1252, 1102,
+    989, 1100, 1252, 1155, 1252, 1142, 1202, 1266, 1337, 1337, 1337, 1310, 1229, 1277, 1229,
+    1277, 1277, 1274, 1416, 1355, 1324, 1181, 1138, 1181, 1225, 1287, 1225, 1399, 1268, 1297,
+    1324, 1268, 1324, 1324, 1203, 1181, 1181, 1225, 1225, 1395, 1225, 1268, 1324, 1245, 1268,
+    1161, 1324, 1138, 1181, 1225, 1225, 1268, 1324, 1324, 1225, 1181, 1290, 1324, 1268, 1414,
+    1526, 1573, 1548, 1620, 1716, 1637, 1685, 1685, 1685, 1801, 1833, 1801, 1796, 1749, 1749,
+    1714, 1526, 1573, 1546, 1620, 1685, 1620, 1685, 1685, 1685, 1893, 1627, 1854, 1801, 1749,
+    1749, 1749, 1556, 1509, 1556, 1603, 1603, 1639, 1603, 1650, 1749, 1749, 1650, 1855, 1749,
+    1486, 1509, 1556, 1603, 1603, 1603, 1603, 1588, 1749, 1749, 1650, 1749, 1761, 1815, 1787,
+    1947, 1755, 1849, 1804, 1849, 1736, 1843, 1948, 1829, 2034, 1948, 1824, 1921, 1921, 1728,
+    1781, 1781, 1815, 1843, 1815, 1749, 1863, 1883, 1921, 1938, 1883, 1981, 1781, 1753, 1812,
+    1815, 1815, 1815, 1821, 1755, 1883, 1921, 1854, 1860, 1964, 1781, 1754, 1781, 1815, 1815,
+    1698, 1815, 1836, 1883, 1921, 1854, 1883, 1921,
 )
 
 ALL = ("all",)
@@ -90,11 +92,13 @@
 
     for stage in range(2):
         base = 10 * stage
-        orders = (("x", "y"), ("x", "y"), ("y", "x"), ("y", "x") if stage == 0 else ("x", "y"))
+        orders = (("x", "y"), ("x", "y"), ("y", "x"), ("y", "x"))
         for quarter, (first, second) in enumerate(orders):
             if quarter == 3:
                 over = [add(quarter, "zd", {}, [], base, 1)]
                 for far in range(2):
+                    if far and stage == 0:
+                        first, second = second, first
                     z = {"z": rel(far)}
                     start = over if far else []
                     plus = add(quarter, first + "+", z, start, base + far, 1)
@@ -134,7 +138,8 @@
                 mo = add(quarter, back, {first: half(1), second: rel(1)}, [ma], base + 4, 2)
                 add(quarter, "zd", {first: ALL, second: rel(-1)}, [pa, pb], base + 5, 4)
                 add(quarter, "zd", {first: ALL, second: rel(1)}, [ma, mb], base + 5, 4)
-                add(quarter, "zd", {first: ALL, second: rel(2)}, [po, mo], base + 6, 4)
+                final = "zw" if stage == 3 else "zd"
+                add(quarter, final, {first: ALL, second: rel(2)}, [po, mo], base + 6, 4)
             else:
                 here, there = {first: ALL}, {first: ALL, "z": rel(1)}
                 ph = add(quarter, forth, here, line, base + 3, 4)
@@ -172,7 +177,8 @@
                 soon = "zw" if stage == 2 and quarter == 0 else "zd"
                 add(quarter, soon, {first: ALL, second: rel(-1)}, [pa, pb], base + 5, 4)
                 add(quarter, "zd", {first: ALL, second: rel(1)}, [ma, mb], base + 5, 4)
-                add(quarter, "zd", {first: ALL, second: rel(2)}, [po, mo], base + 6, 4)
+                final = "zw" if stage == 3 else "zd"
+                add(quarter, final, {first: ALL, second: rel(2)}, [po, mo], base + 6, 4)
             else:
                 over = [
                     add(quarter, way, {first: rel(k)}, needs, base + 2, 1)
@@ -210,8 +216,9 @@
     out += [("mix", k, 1.3 if k % 3 == 2 else 0.7, []) for k in range(6, 12)]
     out += [("home", k, 1.0, []) for k in range(2)]
     out += [("again", k, 1.4, kind("home") + kind("sum", k)) for k in range(2)]
-    out += [("hide", k, 0.72, kind("again") + stage(2)) for k in range(11)]
-    out += [("down", k, 1.5, [s for s in last if near(s)]) for k in range(2)]
+    out += [("pre", k, 0.4, kind("again") + [s for s in stage(2) if near(s)]) for k in range(11)]
+    out += [("hide", k, 0.42, stage(2)) for k in range(11)]
+    out += [("down", 0, 2.1, [s for s in last if near(s)])]
     out += [("down", k, 1.5, last) for k in range(2, 4)]
     return out
 
@@ -334,7 +341,7 @@
 def kernel(
     tokens, gain_one, w_b, w_c, w_v, taps, w_mix, gain_two, w_g, w_u, w_d, total, came_two,
     s0, s1, s2, s3, raw, normed, gated, to_mate, from_mate, summed, mate_sum, to_home, from_home,
-    resid, hidden, gain_v, taps_v, gain_two_v, acc_b, acc_c, local_sem, send_sem, recv_sem,
+    resid, partial, hidden, gain_v, taps_v, gain_two_v, acc_b, acc_c, local_sem, send_sem, recv_sem,
 ):
     sends, steps, _ = plan()
     buffers = (s0, s1, s2, s3)
@@ -411,7 +418,7 @@
         if send.kind == "home":
             return to_home.at[:, cols], from_home.at[:, cols]
         if send.kind == "again":
-            where = normed.at[0, rows_of(core, 160 * j, 160), :]
+            where = normed.at[rows_of(core, 160 * j, 160), :]
             return where, where
         lanes = half_of(j, place["z"])
         return to_mate.at[:, lanes], came_two.at[:, lanes]
@@ -446,11 +453,19 @@
         if step == 0:
             locals_[7].wait()
             locals_[8].wait()
+        if step == 4:
+            for i, send in enumerate(sends):
+                if send.kind == "relay":
+                    outgoing(i).wait_send()
         gain = gain_v[...]
 
         def chunk(r, carry):
             rows = pl.ds(pl.multiple_of(r * 32, 32), 32)
-            normed[c, rows, :] = scaled(raw[c, rows, :].astype(F32), gain)
+            values = scaled(raw[c, rows, :].astype(F32), gain)
+            if c == 0:
+                normed[rows, :] = values
+            else:
+                raw[c, rows, :] = values
             return carry
 
         lax.fori_loop(5 * part, 5 * part + 5, chunk, 0)
@@ -462,7 +477,8 @@
 
         def dot(k):
             w = s0[:, :, :, :, pl.ds(512 * k + 256 * j, 256)].reshape(D, 256)
-            return jnp.dot(normed[c], w, preferred_element_type=F32).astype(BF16)
+            left = raw[1] if c == 1 else normed[...]
+            return jnp.dot(left, w, preferred_element_type=F32).astype(BF16)
 
         if k < 2:
             (acc_b, acc_c)[k][...] = dot(k)
@@ -515,23 +531,37 @@
             sums = sums + mate_sum[rows, :].astype(F32)
             values = raw[0, here, :].astype(F32) + sums
             resid[rows, :] = values
-            normed[0, here, :] = scaled(values, gain)
+            normed[here, :] = scaled(values, gain)
             return carry
 
         lax.fori_loop(0, 5, chunk, 0)
 
+    def half_product(k, plane):
+        w_gate = s2[plane, :, :, :, pl.ds(128 * k, 128)].reshape(D // 2, 128)
+        w_up = s2[plane, :, :, :, pl.ds(1408 + 128 * k, 128)].reshape(D // 2, 128)
+        left = normed[:, pl.ds(pl.multiple_of(1024 * plane, 1024), 1024)]
+        return jnp.dot(
+            left, jnp.concatenate([w_gate, w_up], axis=1), preferred_element_type=F32
+        )
+
+    def pre(k):
+        partial[k] = half_product(k, zl)
+
     def hide(k):
-        w_gate = s2[:, :, :, :, pl.ds(128 * k, 128)].reshape(D, 128)
-        w_up = s2[:, :, :, :, pl.ds(1408 + 128 * k, 128)].reshape(D, 128)
-        both = jnp.dot(
-            normed[0], jnp.concatenate([w_gate, w_up], axis=1), preferred_element_type=F32
-        )
+        both = partial[k] + half_product(k, 1 - zl)
         gate, up = both[:, :128], both[:, 128:]
         hidden[:, pl.ds(128 * k, 128)] = (gate / (1.0 + jnp.exp(-gate)) * up).astype(BF16)
 
     def down(step):
         j = step // 2
         plane = lax.rem(zl + j, 2)
+
+        def both(k, carry):
+            cols = pl.ds(pl.multiple_of(1024 * plane + 256 * k, 256), 256)
+            acc_b[...] = block(hidden[...], s3[plane, k].reshape(256, 1408)).astype(BF16)
+            to_mate[:, cols] = acc_b[other, :]
+            total[:, cols] = resid[:, cols] + 0.5 * acc_b[mine, :].astype(F32)
+            return carry
 
         def theirs(k, carry):
             cols = pl.ds(pl.multiple_of(1024 * plane + 256 * k, 256), 256)
@@ -549,14 +579,11 @@
             for i, send in enumerate(sends):
                 if send.kind == "mate":
                     outgoing(i).wait_send()
-        if step % 2 == 0:
-            lax.fori_loop(0, 4, theirs, 0)
-        else:
-            lax.fori_loop(0, 4, ours, 0)
+        lax.fori_loop(0, 4, (both, None, theirs, ours)[step], 0)
 
     act = {
         "norm": norm, "mix": mix, "mate": mate, "sum": add_up, "home": home, "again": again,
-        "hide": hide, "down": down,
+        "pre": pre, "hide": hide, "down": down,
     }
     landed = set()
     for what, i in steps:
@@ -573,7 +600,7 @@
             act[what](i)
 
     for i, send in enumerate(sends):
-        if send.kind != "mate":
+        if send.kind not in ("mate", "relay"):
             outgoing(i).wait_send()
 
 
@@ -591,10 +618,11 @@
         scratch_shapes=[
             *[pltpu.VMEM((2, 4, 4, 64, width), BF16) for width in WIDTHS],
             pltpu.VMEM((2, T, D), BF16),
-            pltpu.VMEM((2, T, D), BF16),
+            pltpu.VMEM((T, D), BF16),
             pltpu.VMEM((2, T, 512), BF16),
             *[pltpu.VMEM((H, D), BF16)] * 6,
             pltpu.VMEM((H, D), F32),
+            pltpu.VMEM((11, T, 256), F32),
             pltpu.VMEM((T, 1408), BF16),
             pltpu.VMEM((1, D), F32),
             pltpu.VMEM((3, D), F32),

time: 125 us -> 123 us (0.984)
  Pallas kernels: 124 us -> 121 us
    pallas_call x1, Pallas kernels: 124 us -> 121 us  [on_device(): pl.pallas_call(kernel, name='residual_block', out_shape=(pltpu.VMEM((H, D...]
where the time goes in v6:
time: 123 us
  Pallas kernels  121 us (98%)
  other arithmetic  1.48 us (1%)
    pallas_call x1, Pallas kernels, on_device(): pl.pallas_call(kernel, name='residual_block', out_shape=(pltpu.VMEM((H, D...  121 us

profile of v6, /device:TPU:1, one launch (start us, length us, event | category | flops | bytes accessed | tf_op | source)
XLA Modules:
  0.0 122.9 jit_solution(15624135201544004144)
XLA Ops:
  0.0 121.4 %residual_block.1 = (f32[320,2048]{1,0:T(8,128)S(1)}, bf16[320,2048]{1,0:T(8,128)(2,1)S(1)}) custom-call(bf16[320,2048]{1,0:T(8,128)(2,1)} %tokens.1, f32[1,2048]{1,0:T(1,128)} %bitcast.6, bf16[64,1024]{1,0:T(8,128)(2,1)} %w_b.1, bf16[64,1024]{1,0:T(8,128)(2,1)} %w_c.1, bf16[64,1024]{1,0:T(8,128)(2,1)} %w_v.1, f32[3,2048]{1,0:T(4,128)} %taps.1, ...), custom_call_target="tpu_custom_call" | custom-call | tf_op jit(solution)/shard_map/residual_block/pallas_call | solution.py:612
  121.4 1.5 %add_convert_fusion = bf16[320,2048]{1,0:T(8,128)(2,1)} fusion(f32[320,2048]{1,0:T(8,128)S(1)} %get-tuple-element.7, bf16[320,2048]{1,0:T(8,128)(2,1)S(1)} %get-tuple-element.8), kind=kLoop, calls=%fused_computation | loop fusion | flops 2621440 | bytes 5242880 | tf_op jit(solution)/shard_map/convert_element_type | solution.py:643

commit v7 on v6

--- a/solution.py
+++ b/solution.py
@@ -21,27 +21,28 @@
 PAIR = 500.0e3
 LATENCY = 3.4
 PAIR_LATENCY = 1.8
-BACKLOG = 2.93
+BACKLOG = 2.95
 HOLD = 0.0
 
 RANKS = (
-    -2, -2, -2, -2, -3, -4, -4, -4, -4, -4, -4, -4, -4, -4, -4, 1002, 1057, 1057, 1292, 1292,
-    1292, 1292, 1113, 1182, 1113, 1182, 1182, 1182, 1252, 1252, 1252, 1198, 988, 946, 1100,
-    1100, 1100, 1140, 1155, 1252, 1252, 1155, 1252, 1246, 988, 1044, 1044, 1100, 1100, 1100,
-    1075, 1155, 1252, 1252, 1155, 1272, 1405, 988, 1044, 1100, 1100, 1155, 1138, 1252, 1102,
-    989, 1100, 1252, 1155, 1252, 1142, 1202, 1266, 1337, 1337, 1337, 1310, 1229, 1277, 1229,
-    1277, 1277, 1274, 1416, 1355, 1324, 1181, 1138, 1181, 1225, 1287, 1225, 1399, 1268, 1297,
-    1324, 1268, 1324, 1324, 1203, 1181, 1181, 1225, 1225, 1395, 1225, 1268, 1324, 1245, 1268,
-    1161, 1324, 1138, 1181, 1225, 1225, 1268, 1324, 1324, 1225, 1181, 1290, 1324, 1268, 1414,
-    1526, 1573, 1548, 1620, 1716, 1637, 1685, 1685, 1685, 1801, 1833, 1801, 1796, 1749, 1749,
-    1714, 1526, 1573, 1546, 1620, 1685, 1620, 1685, 1685, 1685, 1893, 1627, 1854, 1801, 1749,
-    1749, 1749, 1556, 1509, 1556, 1603, 1603, 1639, 1603, 1650, 1749, 1749, 1650, 1855, 1749,
-    1486, 1509, 1556, 1603, 1603, 1603, 1603, 1588, 1749, 1749, 1650, 1749, 1761, 1815, 1787,
-    1947, 1755, 1849, 1804, 1849, 1736, 1843, 1948, 1829, 2034, 1948, 1824, 1921, 1921, 1728,
-    1781, 1781, 1815, 1843, 1815, 1749, 1863, 1883, 1921, 1938, 1883, 1981, 1781, 1753, 1812,
-    1815, 1815, 1815, 1821, 1755, 1883, 1921, 1854, 1860, 1964, 1781, 1754, 1781, 1815, 1815,
-    1698, 1815, 1836, 1883, 1921, 1854, 1883, 1921,
+    -2, -2, -2, -2, -3, -4, -4, -4, -4, 0, 88, 187, 1590, 957, 1545, 184, 423, 493, 24, 812,
+    36, 637, 1224, 670, 757, 0, 0, 0, 0, 68, 0, 691, 400, 571, 1576, 633, 600, 1738, 120, 0,
+    0, 0, 358, 0, 0, 561, 776, 42, 671, 530, 474, 348, 108, 229, 889, 531, 168, 852, 1144,
+    819, 31, 0, 366, 555, 1355, 821, 409, 1017, 1145, 1346, 1295, 2765, 1203, 382, 1016, 608,
+    553, 920, 1731, 1495, 1297, 624, 879, 366, 595, 2046, 412, 957, 776, 873, 1105, 1602,
+    1168, 1061, 1407, 0, 1342, 849, 292, 650, 1034, 1494, 964, 1239, 988, 834, 654, 858, 177,
+    976, 1513, 1131, 0, 732, 669, 727, 248, 1074, 687, 1048, 1010, 1056, 1644, -4, -4, -4, -4,
+    -4, -4, -4, -4, -4, 1832, 2023, 1566, 2106, 2229, 2086, 2079, 2213, 2709, 2195, 3090,
+    2502, 1936, 1397, 2530, 3318, 1319, 1669, 1282, 1291, 1180, 1451, 2163, 2091, 2290, 2416,
+    3194, 2408, 2621, 2022, 2447, 2862, 1054, 1191, 2081, 1579, 1751, 1318, 2660, 1630, 2416,
+    2667, 1884, 2554, 2715, 1209, 829, 1283, 1872, 1569, 2177, 1888, 2460, 2398, 1997, 1737,
+    2884, 1606, 1381, 2229, 1643, 2400, 3414, 2461, 2657, 3025, 2783, 5092, 4152, 4053, 4506,
+    4593, 4308, 3832, 1437, 2203, 1824, 3287, 2864, 4034, 3451, 2958, 3064, 4362, 4200, 4078,
+    4107, 2520, 1039, 1527, 3538, 2839, 3301, 3279, 1794, 2685, 4717, 3921, 2142, 4068, 1247,
+    2118, 1921, 2860, 3493, 3912, 3426, 2120, 2597, 4884, 2976, 2666, 4244,
 )
+
+SPANS = ((0, 160), (160, 96), (256, 64))
 
 ALL = ("all",)
 ME = ("rel", 0)
@@ -85,10 +86,7 @@
     other("swap", "pair", [], -3, H * row, 0)
     for j in range(2):
         other("mate", "pair", [("mate", j)], -4, H * 1024 * 2, j)
-        other("sum", "zw", [("sum", j)], -4, 160 * row, j)
         other("home", "pair", [("home", j)], -4, H * 1024 * 2, j)
-        other("again", "pair", [("again", j)], -4, 160 * row, j)
-        other("down", "pair", [("down", 2 * j)], -4, H * 1024 * 2, j)
 
     for stage in range(2):
         base = 10 * stage
@@ -111,10 +109,10 @@
                     z = z | {first: ALL}
                     plus = add(quarter, second + "+", z, line, base + 3, 4)
                     minus = add(quarter, second + "-", z, line, base + 3, 4)
-                    if far:
-                        add(quarter, second + "-", z | {second: rel(1)}, [minus], base + 4, 4)
-                    else:
-                        add(quarter, second + "+", z | {second: rel(-1)}, [plus], base + 4, 4)
+                    z = {"z": rel(far)}
+                    on, back = z | {second: rel(-1)}, z | {second: rel(1)}
+                    add(quarter, second + "+", on | {first: half(0)}, [plus], base + 4, 2)
+                    add(quarter, second + "-", back | {first: half(1)}, [minus], base + 4, 2)
                 continue
             forth, back = first + "+", first + "-"
             plus = add(quarter, forth, {}, [], base, 1)
@@ -148,6 +146,11 @@
                 mt = add(quarter, back, there, over, base + 4, 4)
                 add(quarter, forth, here | {second: rel(-1)}, [ph], base + 5, 4)
                 add(quarter, back, there | {second: rel(1)}, [mt], base + 5, 4)
+    for j, (_, n) in enumerate(SPANS):
+        other("sum", "zw", [("sum", j)], -4, n * row, j)
+        other("again", "pair", [("again", j)], -4, n * row, j)
+    for j, step in enumerate((0, 2, 3)):
+        other("down", "pair", [("down", step)], -4, H * (512 if j else 1024) * 2, j)
     orders = (("x", "y"), ("y", "x"), ("x", "y"), ("y", "x"))
     for stage in range(2, 4):
         base = 20 + 10 * (stage - 2)
@@ -212,14 +215,15 @@
     out += [("norm", k, 1.0, kind("token") + kind("relay")) for k in range(4, 8)]
     out += [("mix", k, 1.3 if k % 3 == 2 else 0.7, stage(0)) for k in range(6)]
     out += [("mate", k, 1.0, stage(1)) for k in range(2)]
-    out += [("sum", k, 0.7, kind("mate")) for k in range(2)]
+    out += [("sum", k, n / 230, kind("mate")) for k, (_, n) in enumerate(SPANS)]
     out += [("mix", k, 1.3 if k % 3 == 2 else 0.7, []) for k in range(6, 12)]
     out += [("home", k, 1.0, []) for k in range(2)]
-    out += [("again", k, 1.4, kind("home") + kind("sum", k)) for k in range(2)]
+    for k, (_, n) in enumerate(SPANS):
+        out.append(("again", k, n / 115, kind("home") + kind("sum", k)))
     out += [("pre", k, 0.4, kind("again") + [s for s in stage(2) if near(s)]) for k in range(11)]
     out += [("hide", k, 0.42, stage(2)) for k in range(11)]
     out += [("down", 0, 2.1, [s for s in last if near(s)])]
-    out += [("down", k, 1.5, last) for k in range(2, 4)]
+    out += [("down", k, 1.5 if k == 4 else 0.75, last) for k in range(2, 5)]
     return out
 
 
@@ -413,18 +417,16 @@
         if send.kind == "mate":
             return to_mate.at[:, cols], from_mate.at[:, cols]
         if send.kind == "sum":
-            rows = pl.ds(160 * j, 160)
+            rows = pl.ds(*SPANS[j])
             return summed.at[rows, :], mate_sum.at[rows, :]
         if send.kind == "home":
             return to_home.at[:, cols], from_home.at[:, cols]
         if send.kind == "again":
-            where = normed.at[rows_of(core, 160 * j, 160), :]
+            where = normed.at[rows_of(core, *SPANS[j]), :]
             return where, where
-        lanes = half_of(j, place["z"])
+        start = 1024 * lax.rem(place["z"] + (j > 0), 2) + (512 if j == 2 else 0)
+        lanes = pl.ds(pl.multiple_of(start, 512), 512 if j else 1024)
         return to_mate.at[:, lanes], came_two.at[:, lanes]
-
-    def half_of(j, z):
-        return pl.ds(pl.multiple_of(1024 * lax.rem(z + j, 2), 1024), 1024)
 
     def copy_of(i, place, core):
         src, dst = ends(sends[i], place, core)
@@ -512,21 +514,24 @@
         product(0, j, to_home)
 
     def add_up(p):
+        start, n = SPANS[p]
+
         def chunk(r, carry):
-            rows = pl.ds(pl.multiple_of(160 * p + r * 32, 32), 32)
+            rows = pl.ds(pl.multiple_of(start + r * 32, 32), 32)
             summed[rows, :] = (resid[rows, :] + from_mate[rows, :].astype(F32)).astype(BF16)
             return carry
 
-        lax.fori_loop(0, 5, chunk, 0)
+        lax.fori_loop(0, n // 32, chunk, 0)
 
     def again(p):
+        start, n = SPANS[p]
         if p == 0:
             locals_[10].wait()
         gain = gain_two_v[...]
 
         def chunk(r, carry):
-            rows = pl.ds(pl.multiple_of(160 * p + r * 32, 32), 32)
-            here = pl.ds(pl.multiple_of(tp * H + 160 * p + r * 32, 32), 32)
+            rows = pl.ds(pl.multiple_of(start + r * 32, 32), 32)
+            here = pl.ds(pl.multiple_of(tp * H + start + r * 32, 32), 32)
             sums = resid[rows, :] + from_home[rows, :].astype(F32)
             sums = sums + mate_sum[rows, :].astype(F32)
             values = raw[0, here, :].astype(F32) + sums
@@ -534,7 +539,7 @@
             normed[here, :] = scaled(values, gain)
             return carry
 
-        lax.fori_loop(0, 5, chunk, 0)
+        lax.fori_loop(0, n // 32, chunk, 0)
 
     def half_product(k, plane):
         w_gate = s2[plane, :, :, :, pl.ds(128 * k, 128)].reshape(D // 2, 128)
@@ -553,8 +558,7 @@
         hidden[:, pl.ds(128 * k, 128)] = (gate / (1.0 + jnp.exp(-gate)) * up).astype(BF16)
 
     def down(step):
-        j = step // 2
-        plane = lax.rem(zl + j, 2)
+        plane = 1 - zl if step else zl
 
         def both(k, carry):
             cols = pl.ds(pl.multiple_of(1024 * plane + 256 * k, 256), 256)
@@ -579,7 +583,8 @@
             for i, send in enumerate(sends):
                 if send.kind == "mate":
                     outgoing(i).wait_send()
-        lax.fori_loop(0, 4, (both, None, theirs, ours)[step], 0)
+        lo, hi = ((0, 4), None, (0, 2), (2, 4), (0, 4))[step]
+        lax.fori_loop(lo, hi, (both, None, theirs, theirs, ours)[step], 0)
 
     act = {
         "norm": norm, "mix": mix, "mate": mate, "sum": add_up, "home": home, "again": again,

time: 123 us -> 122 us (level)
    pallas_call x1, Pallas kernels: 121 us -> 120 us  [on_device(): pl.pallas_call(kernel, name='residual_block', out_shape=(pltpu.VMEM((H, D...]
where the time goes in v7:
time: 122 us
  Pallas kernels  120 us (98%)
  other arithmetic  1.48 us (1%)
    pallas_call x1, Pallas kernels, on_device(): pl.pallas_call(kernel, name='residual_block', out_shape=(pltpu.VMEM((H, D...  120 us

profile of v7, /device:TPU:1, one launch (start us, length us, event | category | flops | bytes accessed | tf_op | source)
XLA Modules:
  0.0 121.6 jit_solution(9120885020784217357)
XLA Ops:
  0.0 120.1 %residual_block.1 = (f32[320,2048]{1,0:T(8,128)S(1)}, bf16[320,2048]{1,0:T(8,128)(2,1)S(1)}) custom-call(bf16[320,2048]{1,0:T(8,128)(2,1)} %tokens.1, f32[1,2048]{1,0:T(1,128)} %bitcast.6, bf16[64,1024]{1,0:T(8,128)(2,1)} %w_b.1, bf16[64,1024]{1,0:T(8,128)(2,1)} %w_c.1, bf16[64,1024]{1,0:T(8,128)(2,1)} %w_v.1, f32[3,2048]{1,0:T(4,128)} %taps.1, ...), custom_call_target="tpu_custom_call" | custom-call | tf_op jit(solution)/shard_map/residual_block/pallas_call | solution.py:617
  120.1 1.5 %add_convert_fusion = bf16[320,2048]{1,0:T(8,128)(2,1)} fusion(f32[320,2048]{1,0:T(8,128)S(1)} %get-tuple-element.7, bf16[320,2048]{1,0:T(8,128)(2,1)S(1)} %get-tuple-element.8), kind=kLoop, calls=%fused_computation | loop fusion | flops 2621440 | bytes 5242880 | tf_op jit(solution)/shard_map/convert_element_type | solution.py:648

commit v8 on v7

--- a/solution.py
+++ b/solution.py
@@ -590,6 +590,11 @@
         "norm": norm, "mix": mix, "mate": mate, "sum": add_up, "home": home, "again": again,
         "pre": pre, "hide": hide, "down": down,
     }
+    def settle(which):
+        for i, send in enumerate(sends):
+            if which(send):
+                outgoing(i).wait_send()
+
     landed = set()
     for what, i in steps:
         if what == "start":
@@ -603,10 +608,11 @@
             incoming(i).wait_recv()
         else:
             act[what](i)
-
-    for i, send in enumerate(sends):
-        if send.kind not in ("mate", "relay"):
-            outgoing(i).wait_send()
+            if (what, i) == ("down", 0):
+                settle(lambda s: s.kind not in ("mate", "relay", "down") and s.stage != 3)
+            if (what, i) == ("down", 4):
+                settle(lambda s: s.stage == 3)
+    settle(lambda s: s.kind == "down")
 
 
 def on_device(

time: 122 us -> 122 us (level)
  no operation moved by 1% of the time
where the time goes in v8:
time: 122 us
  Pallas kernels  120 us (98%)
  other arithmetic  1.48 us (1%)
    pallas_call x1, Pallas kernels, on_device(): pl.pallas_call(kernel, name='residual_block', out_shape=(pltpu.VMEM((H, D...  120 us

profile of v8, /device:TPU:1, one launch (start us, length us, event | category | flops | bytes accessed | tf_op | source)
XLA Modules:
  0.0 121.5 jit_solution(9109683397756048081)
XLA Ops:
  0.0 120.0 %residual_block.1 = (f32[320,2048]{1,0:T(8,128)S(1)}, bf16[320,2048]{1,0:T(8,128)(2,1)S(1)}) custom-call(bf16[320,2048]{1,0:T(8,128)(2,1)} %tokens.1, f32[1,2048]{1,0:T(1,128)} %bitcast.6, bf16[64,1024]{1,0:T(8,128)(2,1)} %w_b.1, bf16[64,1024]{1,0:T(8,128)(2,1)} %w_c.1, bf16[64,1024]{1,0:T(8,128)(2,1)} %w_v.1, f32[3,2048]{1,0:T(4,128)} %taps.1, ...), custom_call_target="tpu_custom_call" | custom-call | tf_op jit(solution)/shard_map/residual_block/pallas_call | solution.py:623
  120.0 1.5 %add_convert_fusion = bf16[320,2048]{1,0:T(8,128)(2,1)} fusion(f32[320,2048]{1,0:T(8,128)S(1)} %get-tuple-element.7, bf16[320,2048]{1,0:T(8,128)(2,1)S(1)} %get-tuple-element.8), kind=kLoop, calls=%fused_computation | loop fusion | flops 2621440 | bytes 5242880 | tf_op jit(solution)/shard_map/convert_element_type | solution.py:654
